TPU v7x, 32 devices: a whole 2x2x4 slice. The times are simulated.
32 devices in a mesh: ep: 8 (over z, x), tp: 4 (over y, core).
Axes of the slice: x: 2, y: 2, z: 4, core: 2. Of those that a mesh axis runs over, the one named last changes fastest.
Arguments:
- blender_incoming_features: bfloat16 [2048, 4096], P('ep', 'tp'), may hold values from -6 to 6
- entry_latent_matrix: bfloat16 [2048, 2048], P('ep', 'tp'), may hold values from -6 to 6
- exit_latent_matrix: bfloat16 [2048, 2048], P('ep', 'tp'), may hold values from -6 to 6
- unactivated_valve: bfloat16 [2048, 4096], P('ep', 'tp'), may hold values from -6 to 6
- presoftplus_strides: float32 [2048, 64], P('ep', 'tp'), may hold values from -7 to 7
- extra_attenuation: float32 [2048, 64], P('ep', 'tp'), may hold values from -1 to 0
- incoming_feature_kernel: bfloat16 [4, 4096], P(None, 'tp'), may hold values from -3 to 3
- entry_latent_kernel: bfloat16 [4, 2048], P(None, 'tp'), may hold values from -3 to 3
- exit_latent_kernel: bfloat16 [4, 2048], P(None, 'tp'), may hold values from -3 to 3
- stride_offset_vector: float32 [64], P('tp'), may hold values from -1 to 1
- attenuation_speed_exponent: float32 [64], P('tp'), may hold values from -16 to -3
- bypass_coef_vector: float32 [64], P('tp'), may hold values from 0.5 to 4
- cluster_rescale_coefs: bfloat16 [4096], P('tp'), may hold values from 0.099609375 to 1.8984375
- blender_result_matrix: bfloat16 [4096, 2048], P('tp'), may hold values from -0.09375 to 0.09375
- latter_microbatch_activations: bfloat16 [2048, 2048], P('ep'), may hold values from -6 to 6
- specialist_rescale_coefs: bfloat16 [2048], replicated, may hold values from 0.099609375 to 1.8984375
- specialist_valve_matrix: bfloat16 [8, 2048, 4096], P('ep', None, 'tp'), may hold values from -0.125 to 0.125
- specialist_expand_matrix: bfloat16 [8, 2048, 4096], P('ep', None, 'tp'), may hold values from -0.125 to 0.125
- specialist_contract_matrix: bfloat16 [8, 4096, 2048], P('ep', 'tp'), may hold values from -0.125 to 0.125
- specialist_picks: int32 [2048, 2], P('ep'), may hold values from 0 to 7, all different within a row; in each aligned block of 256 rows (0 to 255, 256 to 511, ...) at most 96 rows name the same one
- selected_specialist_coefs: float32 [2048, 2], P('ep'), may hold values from 0.1 to 1
Outputs:
- mixed_a: bfloat16 [2048, 2048], P(('ep', 'tp'))
- mixed_b: bfloat16 [2048, 2048], P('ep', 'tp')
Inputs may be any that keep to these rules, and one draw needn't show every extreme that they name: `specialist_picks`: in each aligned block of 256 rows, the rows of one index of ep, no expert is named by more than 96 rows, a bound that some block reaches.
All inputs are finite; a program needn't handle non-finite values.
Results may differ from a plain program's by a relative error of at most 0.019.
Values may be sent and summed in bfloat16 or wider, within the bound.
A program may use at most 64 MiB of HBM per device.

v0:
```python
import jax
import jax.numpy as jnp
from jax import lax
from jax.sharding import PartitionSpec as P

HEADS = 64
HEAD_DIM = 64
SHARING_CLUSTERS = 16
STATE = 128
BLOCK = 64
TOPK = 2


NORM_EPS = 1e-06
HIGHEST = lax.Precision.HIGHEST


def from_behind(block, axis, distance):
    devices = range(lax.axis_size(axis))
    route = [(i - distance, i) for i in devices if i - distance in devices]
    return lax.ppermute(block, axis, route)


def prefix(x, axis, join, neutral):
    place = lax.axis_index(axis)
    gathered = jax.tree.map(
        lambda a, kind: lax.all_gather(a.astype(kind), axis), x, (jnp.bfloat16, jnp.bfloat16)
    )
    state = jax.tree.map(lambda a, e: jnp.zeros_like(a) + jnp.asarray(e, a.dtype), x, neutral)

    def one(step, state):
        return join(
            state,
            jax.tree.map(
                lambda a, own: lax.dynamic_index_in_dim(a, step, 0, False).astype(own.dtype),
                gathered,
                x,
            ),
        )

    return lax.fori_loop(0, place, one, state)


def conv_silu(inputs, rim_rows, weight):
    tap_count = weight.shape[0]
    context_span = inputs.shape[0]
    joined = jnp.concatenate([rim_rows, inputs], axis=0).astype(jnp.float32)
    kernel = weight.astype(jnp.float32)
    running_total = kernel[0] * joined[0:context_span]
    for offset in range(1, tap_count):
        running_total = running_total + kernel[offset] * joined[offset : offset + context_span]
    return jax.nn.silu(running_total)


def block_step(carry_state, inputs):
    scaled_x, b_block, c_block, log_block = inputs
    context_span = log_block.shape[0]
    running = jnp.cumsum(log_block, axis=0)
    causal = (jnp.arange(context_span)[:, None] >= jnp.arange(context_span)[None, :])[
        :, :, None, None
    ]
    log_gap = running[:, None] - running[None, :]
    weights = jnp.where(causal, jnp.exp(jnp.where(causal, log_gap, 0.0)), 0.0)
    scores = jnp.einsum("lgn,sgn->lsg", c_block, b_block, preferred_element_type=jnp.float32)
    inside = jnp.einsum("lsgj,sgjp->lgjp", scores[..., None] * weights, scaled_x, precision=HIGHEST)
    c_wide = c_block.astype(jnp.float32)
    b_wide = b_block.astype(jnp.float32)
    before = (
        jnp.einsum("lgn,gjpn->lgjp", c_wide, carry_state, precision=HIGHEST)
        * jnp.exp(running)[..., None]
    )
    to_end = jnp.exp(running[-1] - running)
    carry_state = carry_state * jnp.exp(running[-1])[..., None, None] + jnp.einsum(
        "sgn,sgjp->gjpn", b_wide, scaled_x * to_end[..., None], precision=HIGHEST
    )
    return (carry_state, inside + before)


def combine_states(earlier, later):
    early_state, early_log = earlier
    late_state, late_log = later
    return (early_state * jnp.exp(late_log)[..., None, None] + late_state, early_log + late_log)


def local(
    blender_incoming_features,
    entry_latent_matrix,
    exit_latent_matrix,
    unactivated_valve,
    presoftplus_strides,
    extra_attenuation,
    incoming_feature_kernel,
    entry_latent_kernel,
    exit_latent_kernel,
    stride_offset_vector,
    attenuation_speed_exponent,
    bypass_coef_vector,
    cluster_rescale_coefs,
    blender_result_matrix,
    latter_microbatch_activations,
    specialist_rescale_coefs,
    specialist_valve_matrix,
    specialist_expand_matrix,
    specialist_contract_matrix,
    specialist_picks,
    selected_specialist_coefs,
):
    tap_count = incoming_feature_kernel.shape[0]
    tok_rows = blender_incoming_features.shape[0]
    groups_local = entry_latent_matrix.shape[1] // STATE
    members_within_cluster = HEADS // SHARING_CLUSTERS
    tail_start = tok_rows - tap_count + 1
    rim_x, rim_b, rim_c = from_behind(
        (
            blender_incoming_features[tail_start:],
            entry_latent_matrix[tail_start:],
            exit_latent_matrix[tail_start:],
        ),
        "ep",
        1,
    )
    conv_x_out = conv_silu(blender_incoming_features, rim_x, incoming_feature_kernel).reshape(
        tok_rows, groups_local, members_within_cluster, HEAD_DIM
    )
    conv_b_out = (
        conv_silu(entry_latent_matrix, rim_b, entry_latent_kernel)
        .astype(jnp.bfloat16)
        .reshape(tok_rows, groups_local, STATE)
    )
    conv_c_out = (
        conv_silu(exit_latent_matrix, rim_c, exit_latent_kernel)
        .astype(jnp.bfloat16)
        .reshape(tok_rows, groups_local, STATE)
    )
    stride_amount = jax.nn.softplus(presoftplus_strides + stride_offset_vector[None, :])
    attenuation_exponent = (
        -jnp.exp(attenuation_speed_exponent)[None, :] * stride_amount + extra_attenuation
    ).reshape(tok_rows, groups_local, members_within_cluster)
    scaled_x = (
        conv_x_out
        * stride_amount.reshape(tok_rows, groups_local, members_within_cluster)[..., None]
    )
    blocks = tok_rows // BLOCK

    def as_blocks(array_value):
        return array_value.reshape((blocks, BLOCK) + array_value.shape[1:])

    start_state = jnp.zeros((groups_local, members_within_cluster, HEAD_DIM, STATE), jnp.float32)
    end_state, block_out = lax.scan(
        block_step,
        start_state,
        (
            as_blocks(scaled_x),
            as_blocks(conv_b_out),
            as_blocks(conv_c_out),
            as_blocks(attenuation_exponent),
        ),
    )
    running = jnp.cumsum(attenuation_exponent, axis=0)
    enter_state = prefix(
        (end_state, running[-1]),
        "ep",
        combine_states,
        (jnp.zeros_like(end_state), jnp.zeros_like(running[-1])),
    )[0]
    carried = (
        jnp.einsum("lgn,gjpn->lgjp", conv_c_out.astype(jnp.float32), enter_state, precision=HIGHEST)
        * jnp.exp(running)[..., None]
    )
    ssd_out = (
        block_out.reshape(tok_rows, groups_local, members_within_cluster, HEAD_DIM)
        + carried
        + bypass_coef_vector.reshape(groups_local, members_within_cluster)[None, :, :, None]
        * conv_x_out
    )
    gated_out = ssd_out.reshape(tok_rows, -1) * jax.nn.silu(unactivated_valve.astype(jnp.float32))
    grouped = gated_out.reshape(tok_rows, groups_local, -1)
    grouped = grouped * lax.rsqrt(jnp.mean(grouped * grouped, axis=-1, keepdims=True) + NORM_EPS)
    normed = (grouped.reshape(tok_rows, -1) * cluster_rescale_coefs.astype(jnp.float32)).astype(
        jnp.bfloat16
    )
    mixed_a = lax.psum_scatter(
        jnp.dot(normed, blender_result_matrix, preferred_element_type=jnp.float32).astype(
            jnp.bfloat16
        ),
        "tp",
        scatter_dimension=0,
        tiled=True,
    )
    ep_count = lax.axis_size("ep")
    token_count = latter_microbatch_activations.shape[0]
    model_width = latter_microbatch_activations.shape[1]
    local_experts = specialist_valve_matrix.shape[0]
    expert_count = ep_count * local_experts
    capacity = 3 * token_count * TOPK // (2 * expert_count)
    slot_total = expert_count * capacity
    widened = latter_microbatch_activations.astype(jnp.float32)
    normed_b = (
        widened
        * lax.rsqrt(jnp.mean(widened * widened, axis=-1, keepdims=True) + NORM_EPS)
        * specialist_rescale_coefs.astype(jnp.float32)
    ).astype(jnp.bfloat16)
    flat_routes = specialist_picks.reshape(-1)
    assigned = flat_routes.shape[0]
    positions = jnp.arange(assigned, dtype=jnp.int32)
    earlier_same = (flat_routes[:, None] == flat_routes[None, :]) & (
        positions[None, :] < positions[:, None]
    )
    slot_rank = jnp.sum(earlier_same.astype(jnp.int32), axis=1)
    slot_of = flat_routes * capacity + slot_rank
    slot_ids = jnp.arange(slot_total, dtype=jnp.int32)
    placing = (slot_ids[:, None] == slot_of[None, :]).astype(jnp.bfloat16)
    placing = jnp.sum(placing.reshape(slot_total, token_count, TOPK), axis=2)
    outgoing = jnp.dot(placing, normed_b, preferred_element_type=jnp.float32).astype(jnp.bfloat16)
    outgoing = outgoing.reshape(ep_count, local_experts, capacity, model_width)
    arrived = lax.all_to_all(outgoing, "ep", split_axis=0, concat_axis=0, tiled=True)
    gate_sum = jnp.einsum(
        "sejd,edf->sejf", arrived, specialist_valve_matrix, preferred_element_type=jnp.float32
    )
    up_sum = jnp.einsum(
        "sejd,edf->sejf", arrived, specialist_expand_matrix, preferred_element_type=jnp.float32
    )
    hidden = (jax.nn.silu(gate_sum) * up_sum).astype(jnp.bfloat16)
    partial_out = jnp.einsum(
        "sejf,efd->sejd", hidden, specialist_contract_matrix, preferred_element_type=jnp.float32
    )
    summed = lax.psum_scatter(
        partial_out.astype(jnp.bfloat16), "tp", scatter_dimension=3, tiled=True
    )
    returned = lax.all_to_all(summed, "ep", split_axis=0, concat_axis=0, tiled=True)
    returned = returned.reshape(slot_total, -1)
    token_slots = slot_of.reshape(token_count, TOPK)
    combined = jnp.zeros((token_count, returned.shape[1]), jnp.float32)
    for pick_index in range(TOPK):
        selecting = (token_slots[:, pick_index][:, None] == slot_ids[None, :]).astype(jnp.bfloat16)
        chosen_rows = jnp.dot(selecting, returned, preferred_element_type=jnp.float32)
        combined = combined + chosen_rows * selected_specialist_coefs[:, pick_index][:, None]
    mixed_b = combined.astype(jnp.bfloat16)
    return (mixed_a, mixed_b)


def solution(mesh):
    in_specs = (
        P("ep", "tp"),
        P("ep", "tp"),
        P("ep", "tp"),
        P("ep", "tp"),
        P("ep", "tp"),
        P("ep", "tp"),
        P(None, "tp"),
        P(None, "tp"),
        P(None, "tp"),
        P("tp"),
        P("tp"),
        P("tp"),
        P("tp"),
        P("tp", None),
        P("ep", None),
        P(),
        P("ep", None, "tp"),
        P("ep", None, "tp"),
        P("ep", "tp", None),
        P("ep", None),
        P("ep", None),
    )
    out_specs = (P(("ep", "tp"), None), P("ep", "tp"))
    return jax.shard_map(local, mesh=mesh, in_specs=in_specs, out_specs=out_specs, check_vma=False)
```

profile of v0, /device:TPU:0, one launch (start us, length us, event | category | flops | bytes accessed | tf_op | source)
XLA Modules:
  0.0 228.8 jit_solution(16228402776155507524)
XLA Ops:
  8.0 0.7 slice.108
  8.7 4.9 %collective-permute-start = (bf16[3,1024]{1,0:T(4,128)(2,1)S(1)}, bf16[3,1024]{1,0:T(4,128)(2,1)S(1)}, u32[]{:S(2)}, u32[]{:S(2)}) collective-permute-start(bf16[3,1024]{1,0:T(4,128)(2,1)S(1)} %slice.108), channel_id=1, source_target_pairs={{0,4},{4,8},{8,12},{12,16},{16,20},{20,24},{24,28},{1,5},{5,9},{9,... | collective-permute-start | bytes 18440 | tf_op jit(solution)/shard_map/ppermute | solution.py:21
  13.6 0.7 slice.117
  14.3 3.4 %collective-permute-start.1 = (bf16[3,512]{1,0:T(4,128)(2,1)S(1)}, bf16[3,512]{1,0:T(4,128)(2,1)S(1)}, u32[]{:S(2)}, u32[]{:S(2)}) collective-permute-start(bf16[3,512]{1,0:T(4,128)(2,1)S(1)} %slice.117), channel_id=1, source_target_pairs={{0,4},{4,8},{8,12},{12,16},{16,20},{20,24},{24,28},{1,5},{5,9},{9,... | collective-permute-start | bytes 9224 | tf_op jit(solution)/shard_map/ppermute | solution.py:21
  17.7 0.7 slice.126
  18.5 3.4 %collective-permute-start.2 = (bf16[3,512]{1,0:T(4,128)(2,1)S(1)}, bf16[3,512]{1,0:T(4,128)(2,1)S(1)}, u32[]{:S(2)}, u32[]{:S(2)}) collective-permute-start(bf16[3,512]{1,0:T(4,128)(2,1)S(1)} %slice.126), channel_id=1, source_target_pairs={{0,4},{4,8},{8,12},{12,16},{16,20},{20,24},{24,28},{1,5},{5,9},{9,... | collective-permute-start | bytes 9224 | tf_op jit(solution)/shard_map/ppermute | solution.py:21
  21.8 0.8 copy.183
  25.0 1.5 fusion.48
  26.5 4.0 %convolution_convert_fusion = bf16[768,2048]{1,0:T(8,128)(2,1)} fusion(bf16[768,256]{1,0:T(8,128)(2,1)S(1)} %fusion.81, bf16[256,2048]{1,0:T(8,128)(2,1)} %param.39, f32[2048]{0:T(1024)S(1)} %convert_element_type.117, f32[256]{0:T(256)S(1)} %add_rsqrt_fusion.1), kind=kOutput, calls=%fused_computation.51 | convolution fusion | flops 808976384 | bytes 4596736 | tf_op jit(solution)/shard_map/dot_general | solution.py:214
  30.6 4.6 %all-to-all-start = ((bf16[8,1,96,2048]{3,2,1,0:T(8,128)(2,1)}), bf16[8,1,96,2048]{3,2,1,0:T(8,128)(2,1)}, u32[]{:S(2)}, u32[]{:S(2)}) async-start(bf16[8,1,96,2048]{3,2,1,0:T(8,128)(2,1)} %bitcast.26), calls=%async_computation.1 | async-start | bytes 6291456 | tf_op jit(solution)/shard_map/all_to_all | solution.py:216
  37.5 0.8 reshape_reshape.10
  38.3 0.8 reshape_reshape.11
  39.9 2.7 %reshape.148 = f32[4,64,4,4,64]{4,3,2,1,0:T(4,128)} reshape(f32[256,1024]{1,0:T(8,128)S(1)} %divide_multiply_fusion) | data formatting | bytes 2097152 | tf_op jit(solution)/shard_map/reshape | solution.py:122
  42.6 3.5 %broadcast_multiply_fusion = f32[4,64,4,4,64]{4,3,2,1,0:T(4,128)} fusion(f32[4,64,4,4,64]{4,3,2,1,0:T(4,128)} %reshape.148, f32[4,64,4,4]{3,2,1,0:T(4,128)S(1)} %copy.167), kind=kLoop, calls=%fused_computation.97 | loop fusion | flops 262144 | bytes 2113536 | tf_op jit(solution)/shard_map/mul | solution.py:140
  46.1 80.5 %while.26 = (s32[]{:T(128)}, f32[4,4,64,128]{3,2,1,0:T(8,128)S(1)}, f32[4,64,4,4,64]{1,0,4,3,2:T(4,128)}, f32[4,64,4,4]{1,0,3,2:T(4,128)}, f32[4,64,4,4,64]{4,3,...) while((s32[]{:T(128)}, f32[4,4,64,128]{3,2,1,0:T(8,128)S(1)}, ...), condition=%wide.region_2.3_spmd.clone, body=%wide.region_0.2_spmd.clone.sunk | while | flops 256905216 | bytes 5325568 | solution.py:149
  46.1 1.1 constant_dynamic-slice_fusion.7
  47.5 0.8 constant_dynamic-slice_fusion.8
  48.6 0.9 constant_dynamic-slice_fusion.9
  49.8 1.1 convolution_bitcast_fusion.7
  52.1 14.2 %dynamic_update_slice.6 = f32[4,64,4,4,64]{1,0,4,3,2:T(4,128)} dynamic-update-slice(f32[4,64,4,4,64]{1,0,4,3,2:T(4,128)} %get-tuple-element.299, f32[1,64,4,4,64]{1,0,4,3,2:T(1,128)S(1)} %bitcast.223, s32[]{:T(128)S(6)} %copy.251, s32[]{:T(128)} %constant.64.clone.1..sunk.1, s32[]{:T(128)} %constant.64.clone.1..sunk.1, s32[]{:T(128)} %constant.64.clone.1..sunk.1, s32[]{:T(128)} %constant.64.clone.1..sunk.1) | dynamic-update-slice | bytes 524292 | tf_op jit(solution)/shard_map/while/body/jit(dynamic_update_index_in_dim)/dynamic_update_slice | solution.py:149
  66.2 1.1 constant_dynamic-slice_fusion.7
  67.6 0.8 constant_dynamic-slice_fusion.8
  68.7 0.9 constant_dynamic-slice_fusion.9
  69.9 1.1 convolution_bitcast_fusion.7
  72.2 14.2 %dynamic_update_slice.6 = f32[4,64,4,4,64]{1,0,4,3,2:T(4,128)} dynamic-update-slice(f32[4,64,4,4,64]{1,0,4,3,2:T(4,128)} %get-tuple-element.299, f32[1,64,4,4,64]{1,0,4,3,2:T(1,128)S(1)} %bitcast.223, s32[]{:T(128)S(6)} %copy.251, s32[]{:T(128)} %constant.64.clone.1..sunk.1, s32[]{:T(128)} %constant.64.clone.1..sunk.1, s32[]{:T(128)} %constant.64.clone.1..sunk.1, s32[]{:T(128)} %constant.64.clone.1..sunk.1) | dynamic-update-slice | bytes 524292 | tf_op jit(solution)/shard_map/while/body/jit(dynamic_update_index_in_dim)/dynamic_update_slice | solution.py:149
  86.4 1.1 constant_dynamic-slice_fusion.7
  87.8 0.8 constant_dynamic-slice_fusion.8
  88.8 0.9 constant_dynamic-slice_fusion.9
  90.1 1.1 convolution_bitcast_fusion.7
  92.3 14.2 %dynamic_update_slice.6 = f32[4,64,4,4,64]{1,0,4,3,2:T(4,128)} dynamic-update-slice(f32[4,64,4,4,64]{1,0,4,3,2:T(4,128)} %get-tuple-element.299, f32[1,64,4,4,64]{1,0,4,3,2:T(1,128)S(1)} %bitcast.223, s32[]{:T(128)S(6)} %copy.251, s32[]{:T(128)} %constant.64.clone.1..sunk.1, s32[]{:T(128)} %constant.64.clone.1..sunk.1, s32[]{:T(128)} %constant.64.clone.1..sunk.1, s32[]{:T(128)} %constant.64.clone.1..sunk.1) | dynamic-update-slice | bytes 524292 | tf_op jit(solution)/shard_map/while/body/jit(dynamic_update_index_in_dim)/dynamic_update_slice | solution.py:149
  106.5 1.1 constant_dynamic-slice_fusion.7
  107.9 0.8 constant_dynamic-slice_fusion.8
  109.0 0.9 constant_dynamic-slice_fusion.9
  110.2 1.1 convolution_bitcast_fusion.7
  112.5 14.2 %dynamic_update_slice.6 = f32[4,64,4,4,64]{1,0,4,3,2:T(4,128)} dynamic-update-slice(f32[4,64,4,4,64]{1,0,4,3,2:T(4,128)} %get-tuple-element.299, f32[1,64,4,4,64]{1,0,4,3,2:T(1,128)S(1)} %bitcast.223, s32[]{:T(128)S(6)} %copy.251, s32[]{:T(128)} %constant.64.clone.1..sunk.1, s32[]{:T(128)} %constant.64.clone.1..sunk.1, s32[]{:T(128)} %constant.64.clone.1..sunk.1, s32[]{:T(128)} %constant.64.clone.1..sunk.1) | dynamic-update-slice | bytes 524292 | tf_op jit(solution)/shard_map/while/body/jit(dynamic_update_index_in_dim)/dynamic_update_slice | solution.py:149
  126.6 0.7 convert_element_type.109
  127.7 8.3 %fusion.32 = f32[8,96,1024]{2,1,0:T(8,128)} fusion(bf16[1,2048,1024]{2,1,0:T(8,128)(2,1)} %param.42, bf16[8,1,96,2048]{3,2,1,0:T(8,128)(2,1)} %all-to-all-done), kind=kOutput, calls=%fused_computation.46 | convolution fusion | flops 3221225472 | bytes 10485760 | tf_op jit(solution)/shard_map/sejd,edf->sejf/dot_general | solution.py:220
  135.9 12.8 %fusion.45 = bf16[8,1,96,2048]{3,2,0,1:T(8,128)(2,1)} fusion(bf16[1,1024,2048]{2,1,0:T(8,128)(2,1)} %param.43, f32[8,96,1024]{2,1,0:T(8,128)} %fusion.32, bf16[1,2048,1024]{2,1,0:T(8,128)(2,1)} %param.41, bf16[8,1,96,2048]{3,2,1,0:T(8,128)(2,1)} %all-to-all-done), kind=kOutput, calls=%fused_computation.61 | convolution fusion | flops 6448742400 | bytes 17825792 | tf_op jit(solution)/shard_map/sejf,efd->sejd/dot_general | solution.py:224
  149.4 4.8 %reduce-window.6 = f32[4,4,2,128]{3,2,1,0:T(2,128)S(1)} reduce-window(f32[4,4,2,128]{3,2,1,0:T(2,128)S(1)} %copy.191, f32[]{:T(128)} %constant.65.clone.1), window={size=1x1x1x128 pad=0_0x0_0x0_0x127_0}, to_apply=%region_3.4 | reduce-window | flops 520192 | bytes 32772 | tf_op jit(solution)/shard_map/reduce-window
  155.1 21.3 %all_gather.10 = bf16[8,4,4]{2,1,0:T(4,128)(2,1)S(1)} all-gather(bf16[1,4,4]{2,1,0:T(4,128)(2,1)S(1)} %slice.169), channel_id=1, replica_groups=mesh['ep'=8,'tp'=4] {'ep'}, dimensions={0}, use_global_device_ids=true | all-gather | bytes 288 | tf_op jit(solution)/shard_map/all_gather | solution.py:27
  176.8 2.5 %reshape.149 = f32[256,4,4,64]{0,3,2,1:T(8,128)S(1)} reshape(f32[4,64,4,4,64]{1,0,4,3,2:T(4,128)} %get-tuple-element.84) | data formatting | bytes 2097152 | tf_op jit(solution)/shard_map/reshape | solution.py:171
  179.4 1.7 fusion.59
  181.1 1.6 copy.180
  182.6 1.3 fusion.96
  185.5 4.6 %convolution_convert_fusion.1 = bf16[256,2048]{1,0:T(8,128)(2,1)} fusion(bf16[1024,2048]{1,0:T(8,128)(2,1)} %param.38, f32[256,1024]{1,0:T(8,128)S(1)} %bitcast.233, f32[1024]{0:T(1024)S(1)} %convert_element_type.111, f32[256,1024]{1,0:T(8,128)S(1)} %copy.180, bf16[256,1024]{1,0:T(8,128)(2,1)S(1)} %copy-done.3), kind=kOutput, calls=%fused_computation.64 | convolution fusion | flops 1076625408 | bytes 7868416 | tf_op jit(solution)/shard_map/dot_general | solution.py:183
  190.2 10.0 %all-to-all-start.1 = ((bf16[8,1,96,512]{3,2,1,0:T(8,128)(2,1)}), bf16[8,1,96,512]{3,2,1,0:T(8,128)(2,1)S(1)}, u32[]{:S(2)}, u32[]{:S(2)}) async-start(bf16[8,1,96,512]{3,2,1,0:T(8,128)(2,1)} %bitcast.235), calls=%async_computation.3 | async-start | bytes 1572864 | tf_op jit(solution)/shard_map/all_to_all | solution.py:230
  200.2 19.7 %all-to-all-done.1 = bf16[8,1,96,512]{3,2,1,0:T(8,128)(2,1)S(1)} async-done(((bf16[8,1,96,512]{3,2,1,0:T(8,128)(2,1)}), bf16[8,1,96,512]{3,2,1,0:T(8,128)(2,1)S(1)}, u32[]{:S(2)}, u32[]{:S(2)}) %all-to-all-start.1) | async-done | bytes 786464 | tf_op jit(solution)/shard_map/all_to_all | solution.py:230
  220.3 1.1 fusion.61
  (160 shorter events, 17.4 us)
Async XLA Ops:
  8.7 30.3 %collective-permute-start = (bf16[3,1024]{1,0:T(4,128)(2,1)S(1)}, bf16[3,1024]{1,0:T(4,128)(2,1)S(1)}, u32[]{:S(2)}, u32[]{:S(2)}) collective-permute-start(bf16[3,1024]{1,0:T(4,128)(2,1)S(1)} %slice.108), channel_id=1, source_target_pairs={{0,4},{4,8},{8,12},{12,16},{16,20},{20,24},{24,28},{1,5},{5,9},{9,... | collective-permute-start | bytes 18440 | tf_op jit(solution)/shard_map/ppermute | solution.py:21
  14.3 22.3 %collective-permute-start.1 = (bf16[3,512]{1,0:T(4,128)(2,1)S(1)}, bf16[3,512]{1,0:T(4,128)(2,1)S(1)}, u32[]{:S(2)}, u32[]{:S(2)}) collective-permute-start(bf16[3,512]{1,0:T(4,128)(2,1)S(1)} %slice.117), channel_id=1, source_target_pairs={{0,4},{4,8},{8,12},{12,16},{16,20},{20,24},{24,28},{1,5},{5,9},{9,... | collective-permute-start | bytes 9224 | tf_op jit(solution)/shard_map/ppermute | solution.py:21
  18.5 18.6 %collective-permute-start.2 = (bf16[3,512]{1,0:T(4,128)(2,1)S(1)}, bf16[3,512]{1,0:T(4,128)(2,1)S(1)}, u32[]{:S(2)}, u32[]{:S(2)}) collective-permute-start(bf16[3,512]{1,0:T(4,128)(2,1)S(1)} %slice.126), channel_id=1, source_target_pairs={{0,4},{4,8},{8,12},{12,16},{16,20},{20,24},{24,28},{1,5},{5,9},{9,... | collective-permute-start | bytes 9224 | tf_op jit(solution)/shard_map/ppermute | solution.py:21
  30.6 4.7 %copy-start.17 = (f32[16]{0:T(128)S(1)}, f32[16]{0:T(128)}, u32[]{:S(2)}) copy-start(f32[16]{0:T(128)} %param.35) | copy-start | bytes 196
  30.6 4.7 %copy-start.8 = (bf16[4,1024]{1,0:T(4,128)(2,1)S(1)}, bf16[4,1024]{1,0:T(4,128)(2,1)}, u32[]{:S(2)}) copy-start(bf16[4,1024]{1,0:T(4,128)(2,1)} %param.31) | copy-start | bytes 24580
  30.6 4.8 %copy-start.9 = (bf16[4,512]{1,0:T(4,128)(2,1)S(1)}, bf16[4,512]{1,0:T(4,128)(2,1)}, u32[]{:S(2)}) copy-start(bf16[4,512]{1,0:T(4,128)(2,1)} %param.32) | copy-start | bytes 12292
  30.6 4.8 %copy-start.11 = (f32[256,16]{0,1:T(8,128)S(1)}, f32[256,16]{0,1:T(8,128)}, u32[]{:S(2)}) copy-start(f32[256,16]{0,1:T(8,128)} %param.30) | copy-start | bytes 49156
  30.6 4.8 %copy-start.12 = (f32[256,16]{0,1:T(8,128)S(1)}, f32[256,16]{0,1:T(8,128)}, u32[]{:S(2)}) copy-start(f32[256,16]{0,1:T(8,128)} %param.29) | copy-start | bytes 49156
  30.6 4.8 %copy-start.15 = (f32[16]{0:T(128)S(1)}, f32[16]{0:T(128)}, u32[]{:S(2)}) copy-start(f32[16]{0:T(128)} %param.34) | copy-start | bytes 196
  30.6 4.9 %copy-start.10 = (bf16[4,512]{1,0:T(4,128)(2,1)S(1)}, bf16[4,512]{1,0:T(4,128)(2,1)}, u32[]{:S(2)}) copy-start(bf16[4,512]{1,0:T(4,128)(2,1)} %param.33) | copy-start | bytes 12292
  30.6 6.0 %copy-start.4 = (bf16[256,512]{1,0:T(8,128)(2,1)S(1)}, bf16[256,512]{1,0:T(8,128)(2,1)}, u32[]{:S(2)}) copy-start(bf16[256,512]{1,0:T(8,128)(2,1)} %param.26) | copy-start | bytes 786436
  30.6 97.0 %all-to-all-start = ((bf16[8,1,96,2048]{3,2,1,0:T(8,128)(2,1)}), bf16[8,1,96,2048]{3,2,1,0:T(8,128)(2,1)}, u32[]{:S(2)}, u32[]{:S(2)}) async-start(bf16[8,1,96,2048]{3,2,1,0:T(8,128)(2,1)} %bitcast.26), calls=%async_computation.1 | async-start | bytes 6291456 | tf_op jit(solution)/shard_map/all_to_all | solution.py:216
  35.2 1.9 copy-start.5
  35.2 144.1 %all-gather.3.cloned.1.call-start = ((), (), s32[]{:S(2)}) async-start(), calls=%async_computation.6 | async-start | bytes 2359296 | tf_op jit(solution)/shard_map/all_gather | solution.py:27
  35.5 1.6 copy-start.6
  36.7 2.4 %copy-start.2 = (bf16[256,1024]{1,0:T(8,128)(2,1)S(1)}, bf16[256,1024]{1,0:T(8,128)(2,1)}, u32[]{:S(2)}) copy-start(bf16[256,1024]{1,0:T(8,128)(2,1)} %param.25) | copy-start | bytes 1572868
  37.5 1.7 copy-start
  127.4 62.7 %reduce-scatter.5.cloned.1.call-start = ((), (), s32[]{:S(2)}) async-start(), calls=%async_computation.5 | async-start | bytes 3932160 | tf_op jit(solution)/shard_map/reduce_scatter | solution.py:227
  148.7 0.7 copy-start.7
  148.7 6.3 %copy-start.16 = (f32[16]{0:T(128)S(1)}, f32[16]{0:T(128)}, u32[]{:S(2)}) copy-start(f32[16]{0:T(128)} %param.36) | copy-start | bytes 196
  148.7 6.4 %copy-start.13 = (bf16[1024]{0:T(1024)(128)(2,1)S(1)}, bf16[1024]{0:T(1024)(128)(2,1)}, u32[]{:S(2)}) copy-start(bf16[1024]{0:T(1024)(128)(2,1)} %param.37) | copy-start | bytes 6148
  148.7 27.7 %copy-start.1 = (bf16[256,512]{1,0:T(8,128)(2,1)S(1)}, bf16[256,512]{1,0:T(8,128)(2,1)}, u32[]{:S(2)}) copy-start(bf16[256,512]{1,0:T(8,128)(2,1)} %copy-done) | copy-start | bytes 786436
  148.7 72.7 %reduce-scatter.3.cloned.1.call-start = ((), (), s32[]{:S(2)}) async-start(), calls=%async_computation.4 | async-start | bytes 1310720 | tf_op jit(solution)/shard_map/reduce_scatter | solution.py:182
  184.5 1.0 copy-start.3
  185.5 14.6 %copy-start.14 = (f32[256,2]{0,1:T(2,128)S(1)}, f32[256,2]{0,1:T(2,128)}, u32[]{:S(2)}) copy-start(f32[256,2]{0,1:T(2,128)} %param.45) | copy-start | bytes 6148
  190.2 29.7 %all-to-all-start.1 = ((bf16[8,1,96,512]{3,2,1,0:T(8,128)(2,1)}), bf16[8,1,96,512]{3,2,1,0:T(8,128)(2,1)S(1)}, u32[]{:S(2)}, u32[]{:S(2)}) async-start(bf16[8,1,96,512]{3,2,1,0:T(8,128)(2,1)} %bitcast.235), calls=%async_computation.3 | async-start | bytes 1572864 | tf_op jit(solution)/shard_map/all_to_all | solution.py:230
Sparse Core Ops, SparseCore 0:
  127.5 50.4 all-gather.2
Sparse Core Ops, SparseCore 1:
  148.8 38.8 reduce-scatter.4
  190.6 29.6 reduce-scatter.2
where the time goes:
time: 232 us; the launch traced here: 229 us
  local copies, waits for them, and re-layouts  86.9 us (37%)
  matrix products  41.3 us (18%)
  starting transfers between devices  26.6 us (11%)
  blocking collectives  21.3 us (9%)
  waiting for transfers between devices  19.8 us (9%)
  other arithmetic  16.5 us (7%)
  between operations  16 us (7%)
    dynamic_update_slice x4, local copies, waits for them, and re-layouts, local(): lax.scan(block_step, start_state, (as_blocks(scaled_x), as_blocks(conv_b_...  56.6 us
    all_gather x1, blocking collectives, prefix(): lax.all_gather(a.astype(kind), axis)  21.3 us
    all_to_all x1, waiting for transfers between devices, local(): lax.all_to_all(summed, 'ep', split_axis=0, concat_axis=0, tiled=True)  19.7 us
    dynamic_slice x20, local copies, waits for them, and re-layouts, local(): lax.scan(block_step, start_state, (as_blocks(scaled_x), as_blocks(conv_b_...  12.9 us
    dot_general x1, matrix products, local(): jnp.einsum('sejf,efd->sejd', hidden, specialist_contract_matrix, preferre...  12.8 us
    ppermute x3, starting transfers between devices, from_behind(): return lax.ppermute(block, axis, route)  11.7 us
    all_to_all x1, starting transfers between devices, local(): lax.all_to_all(summed, 'ep', split_axis=0, concat_axis=0, tiled=True)  9.97 us
    dot_general x1, matrix products, local(): jnp.einsum('sejd,edf->sejf', arrived, specialist_expand_matrix, preferred...  8.25 us
  transfers between devices with their start and end apart: 8, of which 1 were waited for; matrix products, arithmetic and copies ran while one was open for 63% of the time, Pallas kernels for 0%

commit v1 on v0

v1 whole, which is shorter than its diff:
```python
import functools

import jax
import jax.numpy as jnp
from jax import lax
from jax.experimental import pallas as pl
from jax.experimental.pallas import tpu as pltpu
from jax.sharding import PartitionSpec as P

HEADS = 64
HEAD_DIM = 64
SHARING_CLUSTERS = 16
STATE = 128
BLOCK = 64
TOPK = 2


NORM_EPS = 1e-06
HIGHEST = lax.Precision.HIGHEST


def from_behind(block, axis, distance):
    devices = range(lax.axis_size(axis))
    route = [(i - distance, i) for i in devices if i - distance in devices]
    return lax.ppermute(block, axis, route)


VMEM = pl.BlockSpec(memory_space=pltpu.VMEM)
HALO = 8
LANES = 128


def silu(v):
    return v / (1.0 + jnp.exp(-v))


def widen(per_head, first, count, rows):
    lane = lax.broadcasted_iota(jnp.int32, (rows, LANES), 1)
    pieces = []
    for h in range(first, first + count, 2):
        left = jnp.broadcast_to(per_head[:, h : h + 1], (rows, LANES))
        right = jnp.broadcast_to(per_head[:, h + 1 : h + 2], (rows, LANES))
        pieces.append(jnp.where(lane < HEAD_DIM, left, right))
    return jnp.concatenate(pieces, axis=1)


def ssd_kernel(
    members,
    x_ref,
    b_ref,
    c_ref,
    rim_ref,
    pre_ref,
    extra_ref,
    kx_ref,
    kb_ref,
    kc_ref,
    offset_ref,
    speed_ref,
    bypass_ref,
    y_ref,
    cc_ref,
    run_ref,
    pieces_ref,
    joined,
    state,
):
    rows, channels = x_ref.shape
    latent = b_ref.shape[1]
    groups = latent // STATE
    wide = members * HEAD_DIM
    taps = kx_ref.shape[0]
    ep_count, piece = pieces_ref.shape[0], pieces_ref.shape[1] - 2

    def conv(ref, k_ref, start, width, rim_start):
        joined[0:HALO, 0:width] = rim_ref[:, rim_start : rim_start + width].astype(jnp.float32)
        joined[HALO : HALO + rows, 0:width] = ref[:, start : start + width].astype(jnp.float32)
        kernel = k_ref[:, start : start + width].astype(jnp.float32)
        total = None
        for j in range(taps):
            at = HALO - taps + 1 + j
            term = kernel[j : j + 1] * joined[at : at + rows, 0:width]
            total = term if total is None else total + term
        return silu(total)

    z = pre_ref[...] + offset_ref[...]
    step = jnp.maximum(z, 0.0) + jnp.log1p(jnp.exp(-jnp.abs(z)))
    decay = -jnp.exp(speed_ref[...]) * step + extra_ref[...]
    row = lax.broadcasted_iota(jnp.int32, (rows, rows), 0)
    col = lax.broadcasted_iota(jnp.int32, (rows, rows), 1)
    causal = row >= col
    tri = causal.astype(jnp.float32)
    run = jnp.dot(tri, decay, preferred_element_type=jnp.float32, precision=HIGHEST)
    run_t = lax.dot_general(
        decay,
        tri,
        (((0,), (1,)), ((), ())),
        preferred_element_type=jnp.float32,
        precision=HIGHEST,
    )
    run_ref[...] = run
    last = run[rows - 1 : rows]
    to_end = jnp.exp(last - run)
    bypass = bypass_ref[...]
    lane = lax.broadcasted_iota(jnp.int32, (rows, LANES), 1)
    for g in range(groups):
        first = g * members
        cols = slice(g * wide, (g + 1) * wide)
        xc = conv(x_ref, kx_ref, g * wide, wide, g * wide)
        bb = conv(b_ref, kb_ref, g * STATE, STATE, channels + g * STATE).astype(jnp.bfloat16)
        cc = conv(c_ref, kc_ref, g * STATE, STATE, channels + latent + g * STATE).astype(jnp.bfloat16)
        cc_ref[:, g * STATE : (g + 1) * STATE] = cc
        xs = xc * widen(step, first, members, rows)
        xs16 = xs.astype(jnp.bfloat16)
        scores = lax.dot_general(
            cc, bb, (((1,), (1,)), ((), ())), preferred_element_type=jnp.float32
        )
        scores = jnp.where(causal, scores, 0.0)
        inside = []
        for pair in range(0, members, 2):
            x_pair = xs16[:, pair * HEAD_DIM : (pair + 2) * HEAD_DIM]
            both = []
            for h in (first + pair, first + pair + 1):
                gap = jnp.minimum(run[:, h : h + 1] - run_t[h : h + 1, :], 0.0)
                weights = (jnp.exp(gap) * scores).astype(jnp.bfloat16)
                both.append(jnp.dot(weights, x_pair, preferred_element_type=jnp.float32))
            inside.append(jnp.where(lane < HEAD_DIM, both[0], both[1]))
        y_ref[:, cols] = jnp.concatenate(inside, axis=1) + xc * widen(bypass, first, members, 1)
        x_end = (xs * widen(to_end, first, members, rows)).astype(jnp.bfloat16)
        state[:, cols] = lax.dot_general(
            bb, x_end, (((0,), (0,)), ((), ())), preferred_element_type=jnp.float32
        )
    for e in range(ep_count):
        pieces_ref[e, 0:piece, :] = state[e * piece : (e + 1) * piece, :].astype(jnp.bfloat16)
    logs = widen(last, 0, groups * members, 1)
    high = logs.astype(jnp.bfloat16)
    low = (logs - high.astype(jnp.float32)).astype(jnp.bfloat16)
    for e in range(ep_count):
        pieces_ref[e, piece : piece + 1, :] = high
        pieces_ref[e, piece + 1 : piece + 2, :] = low


def prefix_kernel(in_ref, out_ref):
    ep_count, piece = in_ref.shape[0], in_ref.shape[1] - 2
    entering = jnp.zeros((piece, in_ref.shape[2]), jnp.float32)
    for d in range(ep_count):
        out_ref[d, :, :] = entering.astype(jnp.bfloat16)
        block = in_ref[d, :, :].astype(jnp.float32)
        log = block[piece : piece + 1] + block[piece + 1 : piece + 2]
        entering = entering * jnp.exp(log) + block[0:piece]


def finish_kernel(
    members, y_ref, cc_ref, run_ref, enter_ref, valve_ref, gain_ref, w_ref, out_ref, normed
):
    rows, channels = y_ref.shape
    wide = members * HEAD_DIM

    @pl.when(pl.program_id(0) == 0)
    def _():
        grown = jnp.exp(run_ref[...])
        for g in range(channels // wide):
            cols = slice(g * wide, (g + 1) * wide)
            carried = jnp.dot(
                cc_ref[:, g * STATE : (g + 1) * STATE],
                enter_ref[:, cols],
                preferred_element_type=jnp.float32,
            )
            ssd = y_ref[:, cols] + carried * widen(grown, g * members, members, rows)
            gated = ssd * silu(valve_ref[:, cols].astype(jnp.float32))
            scale = lax.rsqrt(jnp.mean(gated * gated, axis=1, keepdims=True) + NORM_EPS)
            normed[:, cols] = (gated * scale * gain_ref[:, cols].astype(jnp.float32)).astype(
                jnp.bfloat16
            )

    out_ref[...] = jnp.dot(
        normed[...], w_ref[...], preferred_element_type=jnp.float32
    ).astype(jnp.bfloat16)


def experts_kernel(x_ref, gate_ref, up_ref, down_ref, out_ref, total):
    step = pl.program_id(1)
    rows = x_ref[...]
    gate = jnp.dot(rows, gate_ref[...], preferred_element_type=jnp.float32)
    up = jnp.dot(rows, up_ref[...], preferred_element_type=jnp.float32)
    hidden = (silu(gate) * up).astype(jnp.bfloat16)
    term = jnp.dot(hidden, down_ref[...], preferred_element_type=jnp.float32)
    final = pl.num_programs(1) - 1

    @pl.when(step == 0)
    def _():
        total[...] = term

    @pl.when(step > 0)
    def _():
        total[...] += term

    @pl.when(step == final)
    def _():
        out_ref[...] = total[...].astype(jnp.bfloat16)


def run_experts(rows, gate, up, down):
    experts, count, width = rows.shape
    units = gate.shape[2]
    tile = min(256, units)
    return pl.pallas_call(
        experts_kernel,
        grid=(experts, units // tile),
        in_specs=[
            pl.BlockSpec((None, count, width), lambda e, f: (e, 0, 0)),
            pl.BlockSpec((None, width, tile), lambda e, f: (e, 0, f)),
            pl.BlockSpec((None, width, tile), lambda e, f: (e, 0, f)),
            pl.BlockSpec((None, tile, width), lambda e, f: (e, f, 0)),
        ],
        out_specs=pl.BlockSpec((None, count, width), lambda e, f: (e, 0, 0)),
        out_shape=jax.ShapeDtypeStruct((experts, count, width), jnp.bfloat16),
        scratch_shapes=[pltpu.VMEM((count, width), jnp.float32)],
        cost_estimate=pl.CostEstimate(
            flops=6 * experts * count * width * units,
            bytes_accessed=2 * experts * (2 * count * width + 3 * width * units),
            transcendentals=experts * count * units,
        ),
        compiler_params=pltpu.CompilerParams(
            dimension_semantics=("arbitrary", "arbitrary"), vmem_limit_bytes=48 * 1024 * 1024
        ),
        name="experts",
    )(rows, gate, up, down)


def local(
    blender_incoming_features,
    entry_latent_matrix,
    exit_latent_matrix,
    unactivated_valve,
    presoftplus_strides,
    extra_attenuation,
    incoming_feature_kernel,
    entry_latent_kernel,
    exit_latent_kernel,
    stride_offset_vector,
    attenuation_speed_exponent,
    bypass_coef_vector,
    cluster_rescale_coefs,
    blender_result_matrix,
    latter_microbatch_activations,
    specialist_rescale_coefs,
    specialist_valve_matrix,
    specialist_expand_matrix,
    specialist_contract_matrix,
    specialist_picks,
    selected_specialist_coefs,
):
    tap_count = incoming_feature_kernel.shape[0]
    tok_rows = blender_incoming_features.shape[0]
    members_within_cluster = HEADS // SHARING_CLUSTERS
    ep_count = lax.axis_size("ep")
    channels = blender_incoming_features.shape[1]
    latent = entry_latent_matrix.shape[1]
    heads_local = presoftplus_strides.shape[1]
    piece = STATE // ep_count
    tail = tok_rows - HALO
    rim = from_behind(
        jnp.concatenate(
            [
                blender_incoming_features[tail:],
                entry_latent_matrix[tail:],
                exit_latent_matrix[tail:],
            ],
            axis=1,
        ),
        "ep",
        1,
    )
    block_out, conv_c_out, running, pieces = pl.pallas_call(
        functools.partial(ssd_kernel, members_within_cluster),
        in_specs=[VMEM] * 12,
        out_specs=[VMEM] * 4,
        out_shape=[
            jax.ShapeDtypeStruct((tok_rows, channels), jnp.float32),
            jax.ShapeDtypeStruct((tok_rows, latent), jnp.bfloat16),
            jax.ShapeDtypeStruct((tok_rows, heads_local), jnp.float32),
            jax.ShapeDtypeStruct((ep_count, piece + 2, channels), jnp.bfloat16),
        ],
        scratch_shapes=[
            pltpu.VMEM((tok_rows + HALO, members_within_cluster * HEAD_DIM), jnp.float32),
            pltpu.VMEM((STATE, channels), jnp.float32),
        ],
        cost_estimate=pl.CostEstimate(
            flops=2 * tok_rows * tok_rows * channels * 8,
            bytes_accessed=6 * tok_rows * channels * 2,
            transcendentals=tok_rows * tok_rows * heads_local,
        ),
        name="ssd_local",
    )(
        blender_incoming_features,
        entry_latent_matrix,
        exit_latent_matrix,
        rim,
        presoftplus_strides,
        extra_attenuation,
        incoming_feature_kernel,
        entry_latent_kernel,
        exit_latent_kernel,
        stride_offset_vector[None, :],
        attenuation_speed_exponent[None, :],
        bypass_coef_vector[None, :],
    )
    spread = lax.all_to_all(pieces, "ep", split_axis=0, concat_axis=0, tiled=True)
    entering = pl.pallas_call(
        prefix_kernel,
        in_specs=[VMEM],
        out_specs=VMEM,
        out_shape=jax.ShapeDtypeStruct((ep_count, piece, channels), jnp.bfloat16),
        name="state_prefix",
    )(spread)
    enter_state = lax.all_to_all(entering, "ep", split_axis=0, concat_axis=0, tiled=True).reshape(
        STATE, channels
    )
    width_a = blender_result_matrix.shape[1]
    tile_a = min(512, width_a)
    whole = lambda *shape: pl.BlockSpec(shape, lambda i: (0,) * len(shape))
    partial_a = pl.pallas_call(
        functools.partial(finish_kernel, members_within_cluster),
        grid=(width_a // tile_a,),
        in_specs=[
            whole(tok_rows, channels),
            whole(tok_rows, latent),
            whole(tok_rows, heads_local),
            whole(STATE, channels),
            whole(tok_rows, channels),
            whole(1, channels),
            pl.BlockSpec((channels, tile_a), lambda i: (0, i)),
        ],
        out_specs=pl.BlockSpec((tok_rows, tile_a), lambda i: (0, i)),
        out_shape=jax.ShapeDtypeStruct((tok_rows, width_a), jnp.bfloat16),
        scratch_shapes=[pltpu.VMEM((tok_rows, channels), jnp.bfloat16)],
        cost_estimate=pl.CostEstimate(
            flops=2 * tok_rows * channels * (width_a + 4 * STATE),
            bytes_accessed=2 * channels * (width_a + 4 * tok_rows) + 2 * tok_rows * width_a,
            transcendentals=2 * tok_rows * channels,
        ),
        compiler_params=pltpu.CompilerParams(dimension_semantics=("arbitrary",)),
        name="finish_mixer",
    )(
        block_out,
        conv_c_out,
        running,
        enter_state,
        unactivated_valve,
        cluster_rescale_coefs[None, :],
        blender_result_matrix,
    )
    mixed_a = lax.psum_scatter(partial_a, "tp", scatter_dimension=0, tiled=True)
    token_count = latter_microbatch_activations.shape[0]
    model_width = latter_microbatch_activations.shape[1]
    local_experts = specialist_valve_matrix.shape[0]
    expert_count = ep_count * local_experts
    capacity = 3 * token_count * TOPK // (2 * expert_count)
    slot_total = expert_count * capacity
    widened = latter_microbatch_activations.astype(jnp.float32)
    normed_b = (
        widened
        * lax.rsqrt(jnp.mean(widened * widened, axis=-1, keepdims=True) + NORM_EPS)
        * specialist_rescale_coefs.astype(jnp.float32)
    ).astype(jnp.bfloat16)
    flat_routes = specialist_picks.reshape(-1)
    assigned = flat_routes.shape[0]
    positions = jnp.arange(assigned, dtype=jnp.int32)
    earlier_same = (flat_routes[:, None] == flat_routes[None, :]) & (
        positions[None, :] < positions[:, None]
    )
    slot_rank = jnp.sum(earlier_same.astype(jnp.int32), axis=1)
    slot_of = flat_routes * capacity + slot_rank
    slot_ids = jnp.arange(slot_total, dtype=jnp.int32)
    placing = (slot_ids[:, None] == slot_of[None, :]).astype(jnp.bfloat16)
    placing = jnp.sum(placing.reshape(slot_total, token_count, TOPK), axis=2)
    outgoing = jnp.dot(placing, normed_b, preferred_element_type=jnp.float32).astype(jnp.bfloat16)
    outgoing = outgoing.reshape(ep_count, local_experts, capacity, model_width)
    arrived = lax.all_to_all(outgoing, "ep", split_axis=0, concat_axis=0, tiled=True)
    arrived_rows = arrived.transpose(1, 0, 2, 3).reshape(
        local_experts, ep_count * capacity, model_width
    )
    partial_out = run_experts(
        arrived_rows,
        specialist_valve_matrix,
        specialist_expand_matrix,
        specialist_contract_matrix,
    )
    partial_out = partial_out.reshape(local_experts, ep_count, capacity, model_width)
    partial_out = partial_out.transpose(1, 0, 2, 3)
    summed = lax.psum_scatter(
        partial_out, "tp", scatter_dimension=3, tiled=True
    )
    returned = lax.all_to_all(summed, "ep", split_axis=0, concat_axis=0, tiled=True)
    returned = returned.reshape(slot_total, -1)
    token_slots = slot_of.reshape(token_count, TOPK)
    combined = jnp.zeros((token_count, returned.shape[1]), jnp.float32)
    for pick_index in range(TOPK):
        selecting = (token_slots[:, pick_index][:, None] == slot_ids[None, :]).astype(jnp.bfloat16)
        chosen_rows = jnp.dot(selecting, returned, preferred_element_type=jnp.float32)
        combined = combined + chosen_rows * selected_specialist_coefs[:, pick_index][:, None]
    mixed_b = combined.astype(jnp.bfloat16)
    return (mixed_a, mixed_b)


def solution(mesh):
    in_specs = (
        P("ep", "tp"),
        P("ep", "tp"),
        P("ep", "tp"),
        P("ep", "tp"),
        P("ep", "tp"),
        P("ep", "tp"),
        P(None, "tp"),
        P(None, "tp"),
        P(None, "tp"),
        P("tp"),
        P("tp"),
        P("tp"),
        P("tp"),
        P("tp", None),
        P("ep", None),
        P(),
        P("ep", None, "tp"),
        P("ep", None, "tp"),
        P("ep", "tp", None),
        P("ep", None),
        P("ep", None),
    )
    out_specs = (P(("ep", "tp"), None), P("ep", "tp"))
    return jax.shard_map(local, mesh=mesh, in_specs=in_specs, out_specs=out_specs, check_vma=False)
```

time: 232 us -> 191 us (0.82); the launches traced: 229 us -> 191 us
  local copies, waits for them, and re-layouts: 86.9 us -> 5.27 us
  blocking collectives: 21.3 us -> 92.8 us
  matrix products: 41.3 us -> 3.89 us
  Pallas kernels: 0 us -> 33.1 us
  starting transfers between devices: 26.6 us -> 10.5 us
  other arithmetic: 16.5 us -> 3.5 us
  waiting for transfers between devices: 19.8 us -> 27.4 us
    all_to_all x0 -> x2, blocking collectives: none -> 92.8 us  [the longest x1 77.9 us: local(): lax.all_to_all(outgoing, 'ep', split_axis=0, concat_axis=0, tiled=True)]
    dynamic_update_slice x4 -> x0, local copies, waits for them, and re-layouts: 56.6 us -> none  [local(): lax.scan(block_step, start_state, (as_blocks(scaled_x), as_blocks(conv_b_...]
    dot_general x20 -> x0, matrix products: 35.7 us -> none  [the longest x1 12.8 us: local(): jnp.einsum('sejf,efd->sejd', hidden, specialist_contract_matrix, preferre...]
    pallas_call x0 -> x4, Pallas kernels: none -> 33.1 us  [the longest x1 17.9 us: run_experts(): pl.pallas_call(experts_kernel, grid=(experts, units // tile), in_specs=[p...]
    all_gather x1 -> x0, blocking collectives: 21.3 us -> none  [prefix(): lax.all_gather(a.astype(kind), axis)]
    dynamic_slice x20 -> x0, local copies, waits for them, and re-layouts: 12.9 us -> none  [local(): lax.scan(block_step, start_state, (as_blocks(scaled_x), as_blocks(conv_b_...]
    ppermute x3 -> x1, starting transfers between devices: 11.7 us -> 3.46 us  [from_behind(): return lax.ppermute(block, axis, route)]
    all_to_all x1, waiting for transfers between devices: 0.01 us -> 7.61 us  [local(): lax.all_to_all(entering, 'ep', split_axis=0, concat_axis=0, tiled=True)]
  transfers between devices with their start and end apart: 8 -> 5, of which waited for: 1 -> 3; matrix products, arithmetic and copies ran while one was open for 63% -> 2% of each run, Pallas kernels for 0% -> 8%
where the time goes in v1:
time: 191 us
  blocking collectives  92.8 us (49%)
  Pallas kernels  33.1 us (17%)
  waiting for transfers between devices  27.4 us (14%)
  between operations  14.2 us (7%)
  starting transfers between devices  10.5 us (5%)
  local copies, waits for them, and re-layouts  5.27 us (3%)
  matrix products  3.89 us (2%)
  other arithmetic  3.5 us (2%)
    all_to_all x1, blocking collectives, local(): lax.all_to_all(outgoing, 'ep', split_axis=0, concat_axis=0, tiled=True)  77.9 us
    all_to_all x1, waiting for transfers between devices, local(): lax.all_to_all(summed, 'ep', split_axis=0, concat_axis=0, tiled=True)  19.7 us
    pallas_call x1, Pallas kernels, run_experts(): pl.pallas_call(experts_kernel, grid=(experts, units // tile), in_specs=[p...  17.9 us
    all_to_all x1, blocking collectives, local(): lax.all_to_all(pieces, 'ep', split_axis=0, concat_axis=0, tiled=True)  14.9 us
    all_to_all x1, waiting for transfers between devices, local(): lax.all_to_all(entering, 'ep', split_axis=0, concat_axis=0, tiled=True)  7.61 us
    pallas_call x1, Pallas kernels, local(): pl.pallas_call(functools.partial(ssd_kernel, members_within_cluster), in_...  6.76 us
    pallas_call x1, Pallas kernels, local(): pl.pallas_call(functools.partial(finish_kernel, members_within_cluster),...  6.61 us
  transfers between devices with their start and end apart: 5, of which 3 were waited for; matrix products, arithmetic and copies ran while one was open for 2% of the time, Pallas kernels for 8%

profile of v1, /device:TPU:0, one launch (start us, length us, event | category | flops | bytes accessed | tf_op | source)
XLA Modules:
  0.0 190.7 jit_solution(8606327289156139284)
XLA Ops:
  7.2 0.0 reduce-scatter.5.cloned.1.call-start
  7.2 0.8 copy.53
  8.0 0.1 eq.59
  8.2 0.3 convert_reduce_fusion
  8.4 0.1 reduce_sum.33
  8.6 0.1 copy.54
  8.7 0.7 multiply_add_fusion
  9.4 0.3 fusion.10
  9.7 0.7 convert_element_type.29
  10.4 1.5 fusion
  11.9 2.4 %convolution_convert_fusion = bf16[768,2048]{1,0:T(8,128)(2,1)S(1)} fusion(bf16[768,256]{1,0:T(8,128)(2,1)S(1)} %fusion.10, bf16[256,2048]{1,0:T(8,128)(2,1)} %param.35, f32[2048]{0:T(1024)S(1)} %convert_element_type.29, f32[256]{0:T(256)S(1)} %add_rsqrt_fusion), kind=kOutput, calls=%fused_computation | convolution fusion | flops 808976384 | bytes 4596736 | tf_op jit(solution)/shard_map/dot_general | solution.py:378
  14.3 77.9 %all_to_all.20 = bf16[8,1,96,2048]{3,2,1,0:T(8,128)(2,1)} all-to-all(bf16[8,1,96,2048]{3,2,1,0:T(8,128)(2,1)S(1)} %bitcast.19), channel_id=1, replica_groups=mesh['ep'=8,'tp'=4] {'ep'}, dimensions={0} | all-to-all | bytes 6291456 | tf_op jit(solution)/shard_map/all_to_all | solution.py:380
  92.1 17.9 %experts.1 = bf16[1,768,2048]{2,1,0:T(8,128)(2,1)} custom-call(bf16[1,768,2048]{2,1,0:T(8,128)(2,1)} %bitcast.20, bf16[1,2048,1024]{2,1,0:T(8,128)(2,1)} %gate_ref.1, bf16[1,2048,1024]{2,1,0:T(8,128)(2,1)} %up_ref.1, bf16[1,1024,2048]{2,1,0:T(8,128)(2,1)} %down_ref.1), custom_call_target="tpu_custom_call" | custom-call | flops 9663676416 | bytes 18874368 | tf_op jit(solution)/shard_map/experts/pallas_call | solution.py:207
  110.1 0.0 slice-start
  110.1 0.0 slice-start.1
  110.1 0.0 slice-start.2
  110.1 0.0 copy-start.1
  110.1 0.0 copy-start.2
  110.1 0.0 reduce-scatter.5.cloned.1.call-update
  110.1 0.7 slice-done
  110.8 0.0 slice-done.1
  110.8 0.0 slice-done.2
  110.8 0.0 copy-start.3
  110.8 3.5 %collective-permute-start = (bf16[8,2048]{1,0:T(8,128)(2,1)S(1)}, bf16[8,2048]{1,0:T(8,128)(2,1)S(1)}, u32[]{:S(2)}, u32[]{:S(2)}) collective-permute-start(bf16[8,2048]{1,0:T(8,128)(2,1)S(1)} %pad_maximum_fusion), channel_id=1, source_target_pairs={{0,4},{4,8},{8,12},{12,16},{16,20},{20,24},{24,28},{1,5},{5,9},{9,... | collective-permute-start | bytes 98312 | tf_op jit(solution)/shard_map/ppermute | solution.py:25
  114.3 0.0 copy-done.1
  114.3 0.8 copy.51.pre_ref
  115.0 0.0 copy-done.2
  115.0 0.7 copy.52.extra_ref
  115.8 0.1 collective-permute-done.rim_ref
  115.8 0.0 copy-start.5
  115.8 0.6 copy-done.5
  116.4 6.8 %ssd_local.1 = (f32[256,1024]{1,0:T(8,128)}, bf16[256,512]{1,0:T(8,128)(2,1)}, f32[256,16]{1,0:T(8,128)}, bf16[8,18,1024]{2,1,0:T(8,128)(2,1)}) custom-call(bf16[256,1024]{1,0:T(8,128)(2,1)} %x_ref.1, bf16[256,512]{1,0:T(8,128)(2,1)} %b_ref.1, bf16[256,512]{1,0:T(8,128)(2,1)} %c_ref.1, bf16[8,2048]{1,0:T(8,128)(2,1)} %copy-done.5, f32[256,16]{1,0:T(8,128)} %copy.51.pre_ref, ...), custom_call_target="tpu_custom_call" | custom-call | flops 1073741824 | bytes 3145728 | tf_op jit(solution)/shard_map/ssd_local/pallas_call | solution.py:275
  123.2 14.9 %all_to_all.21.in_ref = bf16[8,18,1024]{2,1,0:T(8,128)(2,1)} all-to-all(bf16[8,18,1024]{2,1,0:T(8,128)(2,1)} %get-tuple-element.9), channel_id=1, replica_groups=mesh['ep'=8,'tp'=4] {'ep'}, dimensions={0} | all-to-all | bytes 589824 | tf_op jit(solution)/shard_map/all_to_all | solution.py:309
  138.1 1.8 state_prefix.1
  139.9 3.4 %all-to-all-start.1 = ((bf16[8,16,1024]{2,1,0:T(8,128)(2,1)}), bf16[8,16,1024]{2,1,0:T(8,128)(2,1)S(1)}, u32[]{:S(2)}, u32[]{:S(2)}) async-start(bf16[8,16,1024]{2,1,0:T(8,128)(2,1)} %state_prefix.1), calls=%async_computation.1 | async-start | bytes 524288 | tf_op jit(solution)/shard_map/all_to_all | solution.py:317
  143.4 0.0 reduce-scatter.3.cloned.1.call-start
  143.4 0.0 copy-done.3
  143.4 0.6 broadcast_in_dim.11.gain_ref
  144.0 7.6 %all-to-all-done.1 = bf16[8,16,1024]{2,1,0:T(8,128)(2,1)S(1)} async-done(((bf16[8,16,1024]{2,1,0:T(8,128)(2,1)}), bf16[8,16,1024]{2,1,0:T(8,128)(2,1)S(1)}, u32[]{:S(2)}, u32[]{:S(2)}) %all-to-all-start.1) | async-done | bytes 262176 | tf_op jit(solution)/shard_map/all_to_all | solution.py:317
  151.6 0.7 copy-done
  152.3 6.6 %finish_mixer.1 = bf16[256,2048]{1,0:T(8,128)(2,1)} custom-call(f32[256,1024]{1,0:T(8,128)} %get-tuple-element.6.y_ref, bf16[256,512]{1,0:T(8,128)(2,1)} %get-tuple-element.7.cc_ref, f32[256,16]{1,0:T(8,128)} %get-tuple-element.8.run_ref, bf16[128,1024]{1,0:T(8,128)(2,1)} %bitcast.23, bf16[256,1024]{1,0:T(8,128)(2,1)} %valve_ref.1, ...), custom_call_target="tpu_custom_call" | custom-call | flops 1342177280 | bytes 7340032 | tf_op jit(solution)/shard_map/finish_mixer/pallas_call | solution.py:323
  159.0 0.0 reduce-scatter.3.cloned.1.call-update
  159.0 0.0 reduce-scatter.5.cloned.1.call-done
  159.0 3.6 %all-to-all-start.3 = ((bf16[8,1,96,512]{3,2,1,0:T(8,128)(2,1)}), bf16[8,1,96,512]{3,2,1,0:T(8,128)(2,1)S(1)}, u32[]{:S(2)}, u32[]{:S(2)}) async-start(bf16[8,1,96,512]{3,2,1,0:T(8,128)(2,1)} %reduce-scatter.5.cloned.1.call-done), calls=%async_computation.5 | async-start | bytes 1572864 | tf_op jit(solution)/shard_map/all_to_all | solution.py:395
  162.6 0.0 copy-done.4
  162.6 19.7 %all-to-all-done.3 = bf16[8,1,96,512]{3,2,1,0:T(8,128)(2,1)S(1)} async-done(((bf16[8,1,96,512]{3,2,1,0:T(8,128)(2,1)}), bf16[8,1,96,512]{3,2,1,0:T(8,128)(2,1)S(1)}, u32[]{:S(2)}, u32[]{:S(2)}) %all-to-all-start.3) | async-done | bytes 786464 | tf_op jit(solution)/shard_map/all_to_all | solution.py:395
  182.3 0.4 convolution_multiply_fusion.1
  182.7 1.1 fusion.5
  (7 shorter events, 0.0 us)
Async XLA Ops:
  7.2 151.8 %reduce-scatter.5.cloned.1.call-start = ((), (), s32[]{:S(2)}) async-start(), calls=%async_computation.7 | async-start | bytes 3932160 | tf_op jit(solution)/shard_map/reduce_scatter | solution.py:392
  110.1 0.7 slice-start
  110.1 0.7 slice-start.1
  110.1 0.7 slice-start.2
  110.1 4.2 %copy-start.1 = (f32[256,16]{0,1:T(8,128)S(1)}, f32[256,16]{0,1:T(8,128)}, u32[]{:S(2)}) copy-start(f32[256,16]{0,1:T(8,128)} %param.25) | copy-start | bytes 49156
  110.1 4.9 %copy-start.2 = (f32[256,16]{0,1:T(8,128)S(1)}, f32[256,16]{0,1:T(8,128)}, u32[]{:S(2)}) copy-start(f32[256,16]{0,1:T(8,128)} %param.26) | copy-start | bytes 49156
  110.8 32.6 %copy-start.3 = (bf16[1024]{0:T(1024)(128)(2,1)S(1)}, bf16[1024]{0:T(1024)(128)(2,1)}, u32[]{:S(2)}) copy-start(bf16[1024]{0:T(1024)(128)(2,1)} %param.33) | copy-start | bytes 6148
  110.8 5.0 %collective-permute-start = (bf16[8,2048]{1,0:T(8,128)(2,1)S(1)}, bf16[8,2048]{1,0:T(8,128)(2,1)S(1)}, u32[]{:S(2)}, u32[]{:S(2)}) collective-permute-start(bf16[8,2048]{1,0:T(8,128)(2,1)S(1)} %pad_maximum_fusion), channel_id=1, source_target_pairs={{0,4},{4,8},{8,12},{12,16},{16,20},{20,24},{24,28},{1,5},{5,9},{9,... | collective-permute-start | bytes 98312 | tf_op jit(solution)/shard_map/ppermute | solution.py:25
  115.8 0.6 copy-start.5
  139.9 11.7 %all-to-all-start.1 = ((bf16[8,16,1024]{2,1,0:T(8,128)(2,1)}), bf16[8,16,1024]{2,1,0:T(8,128)(2,1)S(1)}, u32[]{:S(2)}, u32[]{:S(2)}) async-start(bf16[8,16,1024]{2,1,0:T(8,128)(2,1)} %state_prefix.1), calls=%async_computation.1 | async-start | bytes 524288 | tf_op jit(solution)/shard_map/all_to_all | solution.py:317
  143.4 40.5 %reduce-scatter.3.cloned.1.call-start = ((), (), s32[]{:S(2)}) async-start(), calls=%async_computation.6 | async-start | bytes 1310720 | tf_op jit(solution)/shard_map/reduce_scatter | solution.py:354
  151.6 0.7 copy-start
  152.3 10.2 %copy-start.4 = (f32[256,2]{0,1:T(2,128)S(1)}, f32[256,2]{0,1:T(2,128)}, u32[]{:S(2)}) copy-start(f32[256,2]{0,1:T(2,128)} %param.41) | copy-start | bytes 6148
  159.0 23.3 %all-to-all-start.3 = ((bf16[8,1,96,512]{3,2,1,0:T(8,128)(2,1)}), bf16[8,1,96,512]{3,2,1,0:T(8,128)(2,1)S(1)}, u32[]{:S(2)}, u32[]{:S(2)}) async-start(bf16[8,1,96,512]{3,2,1,0:T(8,128)(2,1)} %reduce-scatter.5.cloned.1.call-done), calls=%async_computation.5 | async-start | bytes 1572864 | tf_op jit(solution)/shard_map/all_to_all | solution.py:395
Sparse Core Ops, SparseCore 0:
  110.2 36.7 reduce-scatter.4
  159.1 23.6 reduce-scatter.2

commit v2 on v1

--- a/solution.py
+++ b/solution.py
@@ -180,9 +180,13 @@
 
 def experts_kernel(x_ref, gate_ref, up_ref, down_ref, out_ref, total):
     step = pl.program_id(1)
-    rows = x_ref[...]
-    gate = jnp.dot(rows, gate_ref[...], preferred_element_type=jnp.float32)
-    up = jnp.dot(rows, up_ref[...], preferred_element_type=jnp.float32)
+    parts, _, depth = x_ref.shape
+    gate = up = 0.0
+    for p in range(parts):
+        rows = x_ref[p]
+        deep = slice(p * depth, (p + 1) * depth)
+        gate += jnp.dot(rows, gate_ref[deep, :], preferred_element_type=jnp.float32)
+        up += jnp.dot(rows, up_ref[deep, :], preferred_element_type=jnp.float32)
     hidden = (silu(gate) * up).astype(jnp.bfloat16)
     term = jnp.dot(hidden, down_ref[...], preferred_element_type=jnp.float32)
     final = pl.num_programs(1) - 1
@@ -197,24 +201,26 @@
 
     @pl.when(step == final)
     def _():
-        out_ref[...] = total[...].astype(jnp.bfloat16)
+        for p in range(parts):
+            out_ref[p] = total[:, p * depth : (p + 1) * depth].astype(jnp.bfloat16)
 
 
 def run_experts(rows, gate, up, down):
-    experts, count, width = rows.shape
+    parts, experts, count, depth = rows.shape
+    width = parts * depth
     units = gate.shape[2]
     tile = min(256, units)
     return pl.pallas_call(
         experts_kernel,
         grid=(experts, units // tile),
         in_specs=[
-            pl.BlockSpec((None, count, width), lambda e, f: (e, 0, 0)),
+            pl.BlockSpec((parts, None, count, depth), lambda e, f: (0, e, 0, 0)),
             pl.BlockSpec((None, width, tile), lambda e, f: (e, 0, f)),
             pl.BlockSpec((None, width, tile), lambda e, f: (e, 0, f)),
             pl.BlockSpec((None, tile, width), lambda e, f: (e, f, 0)),
         ],
-        out_specs=pl.BlockSpec((None, count, width), lambda e, f: (e, 0, 0)),
-        out_shape=jax.ShapeDtypeStruct((experts, count, width), jnp.bfloat16),
+        out_specs=pl.BlockSpec((parts, None, count, depth), lambda e, f: (0, e, 0, 0)),
+        out_shape=jax.ShapeDtypeStruct((parts, experts, count, depth), jnp.bfloat16),
         scratch_shapes=[pltpu.VMEM((count, width), jnp.float32)],
         cost_estimate=pl.CostEstimate(
             flops=6 * experts * count * width * units,
@@ -287,7 +293,7 @@
             pltpu.VMEM((STATE, channels), jnp.float32),
         ],
         cost_estimate=pl.CostEstimate(
-            flops=2 * tok_rows * tok_rows * channels * 8,
+            flops=2 * tok_rows * tok_rows * channels * 64,
             bytes_accessed=6 * tok_rows * channels * 2,
             transcendentals=tok_rows * tok_rows * heads_local,
         ),
@@ -306,7 +312,71 @@
         attenuation_speed_exponent[None, :],
         bypass_coef_vector[None, :],
     )
-    spread = lax.all_to_all(pieces, "ep", split_axis=0, concat_axis=0, tiled=True)
+    token_count = latter_microbatch_activations.shape[0]
+    model_width = latter_microbatch_activations.shape[1]
+    local_experts = specialist_valve_matrix.shape[0]
+    expert_count = ep_count * local_experts
+    capacity = 3 * token_count * TOPK // (2 * expert_count)
+    slot_total = expert_count * capacity
+    widened = latter_microbatch_activations.astype(jnp.float32)
+    share = model_width // lax.axis_size("tp")
+    own = lax.axis_index("tp") * share
+    normed_b = (
+        lax.dynamic_slice_in_dim(latter_microbatch_activations, own, share, 1).astype(jnp.float32)
+        * lax.rsqrt(jnp.mean(widened * widened, axis=-1, keepdims=True) + NORM_EPS)
+        * lax.dynamic_slice_in_dim(specialist_rescale_coefs, own, share, 0).astype(jnp.float32)
+    ).astype(jnp.bfloat16)
+    flat_routes = specialist_picks.reshape(-1)
+    assigned = flat_routes.shape[0]
+    positions = jnp.arange(assigned, dtype=jnp.int32)
+    earlier_same = (flat_routes[:, None] == flat_routes[None, :]) & (
+        positions[None, :] < positions[:, None]
+    )
+    slot_rank = jnp.sum(earlier_same.astype(jnp.int32), axis=1)
+    slot_of = flat_routes * capacity + slot_rank
+    slot_ids = jnp.arange(slot_total, dtype=jnp.int32)
+    placing = (slot_ids[:, None] == slot_of[None, :]).astype(jnp.bfloat16)
+    placing = jnp.sum(placing.reshape(slot_total, token_count, TOPK), axis=2)
+    outgoing = jnp.dot(placing, normed_b, preferred_element_type=jnp.float32).astype(jnp.bfloat16)
+    outgoing = outgoing.reshape(ep_count, local_experts, capacity, share)
+    chunks = 2 if capacity % 32 == 0 else 1
+    size = capacity // chunks
+    gathered = []
+    for k in range(chunks):
+        arrived = lax.all_to_all(
+            outgoing[:, :, k * size : (k + 1) * size],
+            "ep",
+            split_axis=0,
+            concat_axis=0,
+            tiled=True,
+        )
+        arrived_rows = arrived.transpose(1, 0, 2, 3).reshape(local_experts, ep_count * size, share)
+        gathered.append(lax.all_gather(arrived_rows, "tp"))
+    spread = None
+    partials = []
+    for k in range(chunks):
+        if spread is None:
+            gathered[k], pieces = lax.optimization_barrier((gathered[k], pieces))
+        else:
+            gathered[k], spread = lax.optimization_barrier((gathered[k], spread))
+        partial_out = run_experts(
+            gathered[k],
+            specialist_valve_matrix,
+            specialist_expand_matrix,
+            specialist_contract_matrix,
+        )
+        if spread is None:
+            partial_out, pieces = lax.optimization_barrier((partial_out, pieces))
+            spread = lax.all_to_all(pieces, "ep", split_axis=0, concat_axis=0, tiled=True)
+        else:
+            partial_out, spread = lax.optimization_barrier((partial_out, spread))
+        partials.append(partial_out)
+    back = []
+    for k in range(chunks):
+        summed = lax.psum_scatter(partials[k], "tp", scatter_dimension=0, tiled=False)
+        summed = summed.reshape(local_experts, ep_count, size, share).transpose(1, 0, 2, 3)
+        back.append(lax.all_to_all(summed, "ep", split_axis=0, concat_axis=0, tiled=True))
+    returned = back[0] if chunks == 1 else jnp.concatenate(back, axis=2)
     entering = pl.pallas_call(
         prefix_kernel,
         in_specs=[VMEM],
@@ -336,7 +406,7 @@
         out_shape=jax.ShapeDtypeStruct((tok_rows, width_a), jnp.bfloat16),
         scratch_shapes=[pltpu.VMEM((tok_rows, channels), jnp.bfloat16)],
         cost_estimate=pl.CostEstimate(
-            flops=2 * tok_rows * channels * (width_a + 4 * STATE),
+            flops=8 * tok_rows * channels * (width_a + 4 * STATE),
             bytes_accessed=2 * channels * (width_a + 4 * tok_rows) + 2 * tok_rows * width_a,
             transcendentals=2 * tok_rows * channels,
         ),
@@ -352,47 +422,6 @@
         blender_result_matrix,
     )
     mixed_a = lax.psum_scatter(partial_a, "tp", scatter_dimension=0, tiled=True)
-    token_count = latter_microbatch_activations.shape[0]
-    model_width = latter_microbatch_activations.shape[1]
-    local_experts = specialist_valve_matrix.shape[0]
-    expert_count = ep_count * local_experts
-    capacity = 3 * token_count * TOPK // (2 * expert_count)
-    slot_total = expert_count * capacity
-    widened = latter_microbatch_activations.astype(jnp.float32)
-    normed_b = (
-        widened
-        * lax.rsqrt(jnp.mean(widened * widened, axis=-1, keepdims=True) + NORM_EPS)
-        * specialist_rescale_coefs.astype(jnp.float32)
-    ).astype(jnp.bfloat16)
-    flat_routes = specialist_picks.reshape(-1)
-    assigned = flat_routes.shape[0]
-    positions = jnp.arange(assigned, dtype=jnp.int32)
-    earlier_same = (flat_routes[:, None] == flat_routes[None, :]) & (
-        positions[None, :] < positions[:, None]
-    )
-    slot_rank = jnp.sum(earlier_same.astype(jnp.int32), axis=1)
-    slot_of = flat_routes * capacity + slot_rank
-    slot_ids = jnp.arange(slot_total, dtype=jnp.int32)
-    placing = (slot_ids[:, None] == slot_of[None, :]).astype(jnp.bfloat16)
-    placing = jnp.sum(placing.reshape(slot_total, token_count, TOPK), axis=2)
-    outgoing = jnp.dot(placing, normed_b, preferred_element_type=jnp.float32).astype(jnp.bfloat16)
-    outgoing = outgoing.reshape(ep_count, local_experts, capacity, model_width)
-    arrived = lax.all_to_all(outgoing, "ep", split_axis=0, concat_axis=0, tiled=True)
-    arrived_rows = arrived.transpose(1, 0, 2, 3).reshape(
-        local_experts, ep_count * capacity, model_width
-    )
-    partial_out = run_experts(
-        arrived_rows,
-        specialist_valve_matrix,
-        specialist_expand_matrix,
-        specialist_contract_matrix,
-    )
-    partial_out = partial_out.reshape(local_experts, ep_count, capacity, model_width)
-    partial_out = partial_out.transpose(1, 0, 2, 3)
-    summed = lax.psum_scatter(
-        partial_out, "tp", scatter_dimension=3, tiled=True
-    )
-    returned = lax.all_to_all(summed, "ep", split_axis=0, concat_axis=0, tiled=True)
     returned = returned.reshape(slot_total, -1)
     token_slots = slot_of.reshape(token_count, TOPK)
     combined = jnp.zeros((token_count, returned.shape[1]), jnp.float32)

time: 191 us -> 169 us (0.88)
  blocking collectives: 92.8 us -> 34.5 us
  waiting for transfers between devices: 27.4 us -> 50 us
  starting transfers between devices: 10.5 us -> 19.5 us
  Pallas kernels: 33.1 us -> 35.7 us
  local copies, waits for them, and re-layouts: 5.27 us -> 7.76 us
    all_to_all x2, blocking collectives: 92.8 us -> 34.5 us  [local(): lax.all_to_all(outgoing[:, :, k * size:(k + 1) * size], 'ep', split_axis=...]
    reduce_scatter x1 -> x2, waiting for transfers between devices: 0.02 us -> 10.3 us  [local(): lax.psum_scatter(partials[k], 'tp', scatter_dimension=0, tiled=False)]
    all_to_all x0 -> x1, waiting for transfers between devices: none -> 9.97 us  [local(): lax.all_to_all(pieces, 'ep', split_axis=0, concat_axis=0, tiled=True)]
    reduce_scatter x1, waiting for transfers between devices: 0.01 us -> 9.06 us  [local(): mixed_a = lax.psum_scatter(partial_a, 'tp', scatter_dimension=0, tiled=True)]
    all_to_all x1 -> x2, waiting for transfers between devices: 19.7 us -> 12.7 us  [local(): lax.all_to_all(summed, 'ep', split_axis=0, concat_axis=0, tiled=True)]
    all_to_all x0 -> x1, starting transfers between devices: none -> 4.72 us  [local(): lax.all_to_all(pieces, 'ep', split_axis=0, concat_axis=0, tiled=True)]
    all_to_all x1 -> x2, starting transfers between devices: 3.56 us -> 7.84 us  [local(): lax.all_to_all(summed, 'ep', split_axis=0, concat_axis=0, tiled=True)]
    unnamed x15 -> x21, local copies, waits for them, and re-layouts: 3.63 us -> 6.71 us
  transfers between devices with their start and end apart: 5 -> 10, of which waited for: 3 -> 7; matrix products, arithmetic and copies ran while one was open for 2% -> 2% of each run, Pallas kernels for 8% -> 21%
where the time goes in v2:
time: 169 us; the launch traced here: 168 us
  waiting for transfers between devices  50 us (30%)
  Pallas kernels  35.7 us (21%)
  blocking collectives  34.5 us (20%)
  starting transfers between devices  19.5 us (12%)
  between operations  14 us (8%)
  local copies, waits for them, and re-layouts  7.76 us (5%)
  other arithmetic  3.63 us (2%)
  matrix products  2.95 us (2%)
    all_to_all x2, blocking collectives, local(): lax.all_to_all(outgoing[:, :, k * size:(k + 1) * size], 'ep', split_axis=...  34.5 us
    pallas_call x2, Pallas kernels, run_experts(): pl.pallas_call(experts_kernel, grid=(experts, units // tile), in_specs=[p...  20.8 us
    all_to_all x2, waiting for transfers between devices, local(): lax.all_to_all(summed, 'ep', split_axis=0, concat_axis=0, tiled=True)  12.7 us
    reduce_scatter x2, waiting for transfers between devices, local(): lax.psum_scatter(partials[k], 'tp', scatter_dimension=0, tiled=False)  10.3 us
    all_to_all x1, waiting for transfers between devices, local(): lax.all_to_all(pieces, 'ep', split_axis=0, concat_axis=0, tiled=True)  9.97 us
    reduce_scatter x1, waiting for transfers between devices, local(): mixed_a = lax.psum_scatter(partial_a, 'tp', scatter_dimension=0, tiled=True)  9.06 us
    all_to_all x2, starting transfers between devices, local(): lax.all_to_all(summed, 'ep', split_axis=0, concat_axis=0, tiled=True)  7.84 us
    all_to_all x1, waiting for transfers between devices, local(): lax.all_to_all(entering, 'ep', split_axis=0, concat_axis=0, tiled=True)  7.81 us
  transfers between devices with their start and end apart: 10, of which 7 were waited for; matrix products, arithmetic and copies ran while one was open for 2% of the time, Pallas kernels for 21%

profile of v2, /device:TPU:0, one launch (start us, length us, event | category | flops | bytes accessed | tf_op | source)
XLA Modules:
  0.0 168.0 jit_solution(4160533942991711649)
XLA Ops:
  7.2 0.0 all-gather.5.cloned.1.call-start
  7.2 0.8 copy.57
  8.0 0.1 eq.60
  8.2 0.3 convert_reduce_fusion
  8.4 0.1 reduce_sum.33
  8.6 0.1 copy.58
  8.7 0.7 multiply_add_fusion
  9.4 0.3 fusion.4
  9.7 1.5 multiply_reduce_fusion
  11.2 0.8 dynamic-slice_convert_fusion
  12.0 1.4 convolution_convert_fusion
  13.4 0.1 fusion.11
  13.5 19.4 %all_to_all.30 = bf16[8,1,48,512]{3,2,1,0:T(8,128)(2,1)} all-to-all(bf16[8,1,48,512]{3,2,1,0:T(8,128)(2,1)S(1)} %get-tuple-element.26), channel_id=1, replica_groups=mesh['ep'=8,'tp'=4] {'ep'}, dimensions={0} | all-to-all | bytes 786432 | tf_op jit(solution)/shard_map/all_to_all | solution.py:346
  32.9 0.0 all-gather.5.cloned.1.call-update
  32.9 0.0 all-gather.3.cloned.1.call-start
  33.0 15.1 %all_to_all.31 = bf16[8,1,48,512]{3,2,1,0:T(8,128)(2,1)} all-to-all(bf16[8,1,48,512]{3,2,1,0:T(8,128)(2,1)S(1)} %get-tuple-element.27), channel_id=1, replica_groups=mesh['ep'=8,'tp'=4] {'ep'}, dimensions={0} | all-to-all | bytes 786432 | tf_op jit(solution)/shard_map/all_to_all | solution.py:346
  48.1 0.0 reduce-scatter.6.cloned.1.call-start
  48.2 3.0 %collective-permute-start = (bf16[8,2048]{1,0:T(8,128)(2,1)S(1)}, bf16[8,2048]{1,0:T(8,128)(2,1)S(1)}, u32[]{:S(2)}, u32[]{:S(2)}) collective-permute-start(bf16[8,2048]{1,0:T(8,128)(2,1)S(1)} %pad_maximum_fusion.1), channel_id=1, source_target_pairs={{0,4},{4,8},{8,12},{12,16},{16,20},{20,24},{24,28},{1,5},{5,9},{9,... | collective-permute-start | bytes 98312 | tf_op jit(solution)/shard_map/ppermute | solution.py:25
  51.2 0.8 copy.55.pre_ref
  51.9 0.8 copy.56.extra_ref
  52.7 0.1 collective-permute-done.rim_ref
  52.8 0.6 copy-done.8
  53.4 6.4 %ssd_local.1 = (f32[256,1024]{1,0:T(8,128)}, bf16[256,512]{1,0:T(8,128)(2,1)}, f32[256,16]{1,0:T(8,128)}, bf16[8,18,1024]{2,1,0:T(8,128)(2,1)}) custom-call(bf16[256,1024]{1,0:T(8,128)(2,1)} %x_ref.1, bf16[256,512]{1,0:T(8,128)(2,1)} %b_ref.1, bf16[256,512]{1,0:T(8,128)(2,1)} %c_ref.1, bf16[8,2048]{1,0:T(8,128)(2,1)} %copy-done.8, f32[256,16]{1,0:T(8,128)} %copy.55.pre_ref, ...), custom_call_target="tpu_custom_call" | custom-call | flops 8589934592 | bytes 3145728 | tf_op jit(solution)/shard_map/ssd_local/pallas_call | solution.py:281
  59.8 1.6 copy-done.1
  61.5 10.3 %experts.2 = bf16[4,1,384,512]{3,2,1,0:T(8,128)(2,1)} custom-call(bf16[4,1,384,512]{3,2,1,0:T(8,128)(2,1)S(1)} %copy-done.1, bf16[1,2048,1024]{2,1,0:T(8,128)(2,1)} %gate_ref.3, bf16[1,2048,1024]{2,1,0:T(8,128)(2,1)} %up_ref.3, bf16[1,1024,2048]{2,1,0:T(8,128)(2,1)} %down_ref.3), custom_call_target="tpu_custom_call" | custom-call | flops 4831838208 | bytes 15728640 | tf_op jit(solution)/shard_map/experts/pallas_call | solution.py:213
  71.8 4.7 %all-to-all-start.2 = ((bf16[8,18,1024]{2,1,0:T(8,128)(2,1)}), bf16[8,18,1024]{2,1,0:T(8,128)(2,1)S(1)}, u32[]{:S(2)}, u32[]{:S(2)}) async-start(bf16[8,18,1024]{2,1,0:T(8,128)(2,1)} %get-tuple-element.20), calls=%async_computation.2 | async-start | bytes 786432 | tf_op jit(solution)/shard_map/all_to_all | solution.py:370
  76.5 0.0 reduce-scatter.8.cloned.1.call-start
  76.6 0.0 all-gather.3.cloned.1.call-done.x_ref
  76.6 10.0 %all-to-all-done.2.in_ref = bf16[8,18,1024]{2,1,0:T(8,128)(2,1)S(1)} async-done(((bf16[8,18,1024]{2,1,0:T(8,128)(2,1)}), bf16[8,18,1024]{2,1,0:T(8,128)(2,1)S(1)}, u32[]{:S(2)}, u32[]{:S(2)}) %all-to-all-start.2) | async-done | bytes 294944 | tf_op jit(solution)/shard_map/all_to_all | solution.py:370
  86.6 1.4 copy-done
  88.0 10.5 %experts.3 = bf16[4,1,384,512]{3,2,1,0:T(8,128)(2,1)} custom-call(bf16[4,1,384,512]{3,2,1,0:T(8,128)(2,1)S(1)} %copy-done, bf16[1,2048,1024]{2,1,0:T(8,128)(2,1)} %gate_ref.3, bf16[1,2048,1024]{2,1,0:T(8,128)(2,1)} %up_ref.3, bf16[1,1024,2048]{2,1,0:T(8,128)(2,1)} %down_ref.3), custom_call_target="tpu_custom_call" | custom-call | flops 4831838208 | bytes 15728640 | tf_op jit(solution)/shard_map/experts/pallas_call | solution.py:213
  98.5 1.8 %state_prefix.1 = bf16[8,16,1024]{2,1,0:T(8,128)(2,1)} custom-call(bf16[8,18,1024]{2,1,0:T(8,128)(2,1)} %copy-done.2), custom_call_target="tpu_custom_call" | custom-call | tf_op jit(solution)/shard_map/state_prefix/pallas_call | solution.py:380
  100.3 3.8 %all-to-all-start.3 = ((bf16[8,16,1024]{2,1,0:T(8,128)(2,1)}), bf16[8,16,1024]{2,1,0:T(8,128)(2,1)S(1)}, u32[]{:S(2)}, u32[]{:S(2)}) async-start(bf16[8,16,1024]{2,1,0:T(8,128)(2,1)} %state_prefix.1), calls=%async_computation.3 | async-start | bytes 524288 | tf_op jit(solution)/shard_map/all_to_all | solution.py:387
  104.0 0.0 reduce-scatter.4.cloned.1.call-start
  104.1 0.6 broadcast_in_dim.11.gain_ref
  104.7 7.8 %all-to-all-done.3 = bf16[8,16,1024]{2,1,0:T(8,128)(2,1)S(1)} async-done(((bf16[8,16,1024]{2,1,0:T(8,128)(2,1)}), bf16[8,16,1024]{2,1,0:T(8,128)(2,1)S(1)}, u32[]{:S(2)}, u32[]{:S(2)}) %all-to-all-start.3) | async-done | bytes 262176 | tf_op jit(solution)/shard_map/all_to_all | solution.py:387
  112.5 0.7 copy-done.3
  113.2 6.7 %finish_mixer.1 = bf16[256,2048]{1,0:T(8,128)(2,1)} custom-call(f32[256,1024]{1,0:T(8,128)} %get-tuple-element.14.y_ref, bf16[256,512]{1,0:T(8,128)(2,1)} %get-tuple-element.15.cc_ref, f32[256,16]{1,0:T(8,128)} %get-tuple-element.16.run_ref, bf16[128,1024]{1,0:T(8,128)(2,1)} %bitcast.31, bf16[256,1024]{1,0:T(8,128)(2,1)} %valve_ref.1, ...), custom_call_target="tpu_custom_call" | custom-call | flops 5368709120 | bytes 7340032 | tf_op jit(solution)/shard_map/finish_mixer/pallas_call | solution.py:393
  119.9 0.0 reduce-scatter.6.cloned.1.call-done
  119.9 3.5 %all-to-all-start.4 = ((bf16[8,1,48,512]{3,2,1,0:T(8,128)(2,1)}), bf16[8,1,48,512]{3,2,1,0:T(8,128)(2,1)S(1)}, u32[]{:S(2)}, u32[]{:S(2)}) async-start(bf16[8,1,48,512]{3,2,1,0:T(8,128)(2,1)} %bitcast.29), calls=%async_computation.6 | async-start | bytes 786432 | tf_op jit(solution)/shard_map/all_to_all | solution.py:378
  123.4 10.3 %reduce-scatter.8.cloned.1.call-done = bf16[1,1,384,512]{3,2,1,0:T(8,128)(2,1)} async-done(((bf16[4,1,384,512]{3,2,1,0:T(8,128)(2,1)}), bf16[1,1,384,512]{3,2,1,0:T(8,128)(2,1)}) %reduce-scatter.8.cloned.1.call-update) | async-done | bytes 393232 | tf_op jit(solution)/shard_map/reduce_scatter | solution.py:376
  133.7 1.1 all-to-all-done.4
  134.8 4.4 %all-to-all-start.5 = ((bf16[8,1,48,512]{3,2,1,0:T(8,128)(2,1)}), bf16[8,1,48,512]{3,2,1,0:T(8,128)(2,1)S(1)}, u32[]{:S(2)}, u32[]{:S(2)}) async-start(bf16[8,1,48,512]{3,2,1,0:T(8,128)(2,1)} %bitcast.30), calls=%async_computation.8 | async-start | bytes 786432 | tf_op jit(solution)/shard_map/all_to_all | solution.py:378
  139.2 11.5 %all-to-all-done.5 = bf16[8,1,48,512]{3,2,1,0:T(8,128)(2,1)S(1)} async-done(((bf16[8,1,48,512]{3,2,1,0:T(8,128)(2,1)}), bf16[8,1,48,512]{3,2,1,0:T(8,128)(2,1)S(1)}, u32[]{:S(2)}, u32[]{:S(2)}) %all-to-all-start.5) | async-done | bytes 393248 | tf_op jit(solution)/shard_map/all_to_all | solution.py:378
  150.7 0.1 pad_maximum_fusion
  150.8 0.4 convolution_multiply_fusion.1
  151.2 1.1 fusion.2
  152.4 9.1 %reduce-scatter.4.cloned.1.call-done = bf16[64,2048]{1,0:T(8,128)(2,1)} async-done(((bf16[256,2048]{1,0:T(8,128)(2,1)}), bf16[64,2048]{1,0:T(8,128)(2,1)}) %reduce-scatter.4.cloned.1.call-update) | async-done | bytes 262160 | tf_op jit(solution)/shard_map/reduce_scatter | solution.py:424
  (29 shorter events, 0.1 us)
Async XLA Ops:
  7.2 52.7 %all-gather.5.cloned.1.call-start = ((), (), s32[]{:S(2)}) async-start(), calls=%async_computation.10 | async-start | bytes 1966080 | tf_op jit(solution)/shard_map/all_gather | solution.py:354
  13.5 34.7 %slice-start = ((bf16[256,1024]{1,0:T(8,128)(2,1)}), bf16[8,1024]{1,0:T(8,128)(2,1)S(1)}, s32[]{:S(2)}) async-start(bf16[256,1024]{1,0:T(8,128)(2,1)} %x_ref.1), calls=%async_computation.14 | async-start | bytes 32768 | tf_op jit(solution)/shard_map/slice | solution.py:272
  13.5 34.7 %slice-start.1 = ((bf16[256,512]{1,0:T(8,128)(2,1)}), bf16[8,512]{1,0:T(8,128)(2,1)S(1)}, s32[]{:S(2)}) async-start(bf16[256,512]{1,0:T(8,128)(2,1)} %c_ref.1), calls=%async_computation.15 | async-start | bytes 16384 | tf_op jit(solution)/shard_map/slice | solution.py:274
  13.5 34.7 %slice-start.2 = ((bf16[256,512]{1,0:T(8,128)(2,1)}), bf16[8,512]{1,0:T(8,128)(2,1)S(1)}, s32[]{:S(2)}) async-start(bf16[256,512]{1,0:T(8,128)(2,1)} %b_ref.1), calls=%async_computation.16 | async-start | bytes 16384 | tf_op jit(solution)/shard_map/slice | solution.py:273
  13.5 37.7 %copy-start.4 = (f32[256,16]{0,1:T(8,128)S(1)}, f32[256,16]{0,1:T(8,128)}, u32[]{:S(2)}) copy-start(f32[256,16]{0,1:T(8,128)} %param.25) | copy-start | bytes 49156
  13.5 38.4 %copy-start.5 = (f32[256,16]{0,1:T(8,128)S(1)}, f32[256,16]{0,1:T(8,128)}, u32[]{:S(2)}) copy-start(f32[256,16]{0,1:T(8,128)} %param.26) | copy-start | bytes 49156
  32.9 43.7 %all-gather.3.cloned.1.call-start = ((), (), s32[]{:S(2)}) async-start(), calls=%async_computation.9 | async-start | bytes 1966080 | tf_op jit(solution)/shard_map/all_gather | solution.py:354
  48.1 71.8 %reduce-scatter.6.cloned.1.call-start = ((), (), s32[]{:S(2)}) async-start(), calls=%async_computation.12 | async-start | bytes 1966080 | tf_op jit(solution)/shard_map/reduce_scatter | solution.py:376
  48.2 4.6 %collective-permute-start = (bf16[8,2048]{1,0:T(8,128)(2,1)S(1)}, bf16[8,2048]{1,0:T(8,128)(2,1)S(1)}, u32[]{:S(2)}, u32[]{:S(2)}) collective-permute-start(bf16[8,2048]{1,0:T(8,128)(2,1)S(1)} %pad_maximum_fusion.1), channel_id=1, source_target_pairs={{0,4},{4,8},{8,12},{12,16},{16,20},{20,24},{24,28},{1,5},{5,9},{9,... | collective-permute-start | bytes 98312 | tf_op jit(solution)/shard_map/ppermute | solution.py:25
  52.8 0.6 copy-start.8
  59.8 1.6 copy-start.1
  71.8 14.8 %all-to-all-start.2 = ((bf16[8,18,1024]{2,1,0:T(8,128)(2,1)}), bf16[8,18,1024]{2,1,0:T(8,128)(2,1)S(1)}, u32[]{:S(2)}, u32[]{:S(2)}) async-start(bf16[8,18,1024]{2,1,0:T(8,128)(2,1)} %get-tuple-element.20), calls=%async_computation.2 | async-start | bytes 786432 | tf_op jit(solution)/shard_map/all_to_all | solution.py:370
  76.5 57.1 %reduce-scatter.8.cloned.1.call-start = ((), (), s32[]{:S(2)}) async-start(), calls=%async_computation.13 | async-start | bytes 1966080 | tf_op jit(solution)/shard_map/reduce_scatter | solution.py:376
  86.6 1.4 copy-start
  88.0 10.5 %copy-start.2 = (bf16[8,18,1024]{2,1,0:T(8,128)(2,1)}, bf16[8,18,1024]{2,1,0:T(8,128)(2,1)S(1)}, u32[]{:S(2)}) copy-start(bf16[8,18,1024]{2,1,0:T(8,128)(2,1)S(1)} %all-to-all-done.2.in_ref) | copy-start | bytes 884740
  98.4 5.6 %copy-start.6 = (bf16[1024]{0:T(1024)(128)(2,1)S(1)}, bf16[1024]{0:T(1024)(128)(2,1)}, u32[]{:S(2)}) copy-start(bf16[1024]{0:T(1024)(128)(2,1)} %param.33) | copy-start | bytes 6148
  100.3 12.2 %all-to-all-start.3 = ((bf16[8,16,1024]{2,1,0:T(8,128)(2,1)}), bf16[8,16,1024]{2,1,0:T(8,128)(2,1)S(1)}, u32[]{:S(2)}, u32[]{:S(2)}) async-start(bf16[8,16,1024]{2,1,0:T(8,128)(2,1)} %state_prefix.1), calls=%async_computation.3 | async-start | bytes 524288 | tf_op jit(solution)/shard_map/all_to_all | solution.py:387
  104.0 57.4 %reduce-scatter.4.cloned.1.call-start = ((), (), s32[]{:S(2)}) async-start(), calls=%async_computation.11 | async-start | bytes 1310720 | tf_op jit(solution)/shard_map/reduce_scatter | solution.py:424
  112.5 0.7 copy-start.3
  119.8 19.3 %copy-start.7 = (f32[256,2]{0,1:T(2,128)S(1)}, f32[256,2]{0,1:T(2,128)}, u32[]{:S(2)}) copy-start(f32[256,2]{0,1:T(2,128)} %param.41) | copy-start | bytes 6148
  119.9 14.9 %all-to-all-start.4 = ((bf16[8,1,48,512]{3,2,1,0:T(8,128)(2,1)}), bf16[8,1,48,512]{3,2,1,0:T(8,128)(2,1)S(1)}, u32[]{:S(2)}, u32[]{:S(2)}) async-start(bf16[8,1,48,512]{3,2,1,0:T(8,128)(2,1)} %bitcast.29), calls=%async_computation.6 | async-start | bytes 786432 | tf_op jit(solution)/shard_map/all_to_all | solution.py:378
  134.8 15.9 %all-to-all-start.5 = ((bf16[8,1,48,512]{3,2,1,0:T(8,128)(2,1)}), bf16[8,1,48,512]{3,2,1,0:T(8,128)(2,1)S(1)}, u32[]{:S(2)}, u32[]{:S(2)}) async-start(bf16[8,1,48,512]{3,2,1,0:T(8,128)(2,1)} %bitcast.30), calls=%async_computation.8 | async-start | bytes 786432 | tf_op jit(solution)/shard_map/all_to_all | solution.py:378
Sparse Core Ops, SparseCore 0:
  33.0 18.3 all-gather.4
  53.0 19.6 all-gather.2
  75.2 27.9 reduce-scatter.5
  105.6 28.0 reduce-scatter.7
  136.6 24.7 reduce-scatter.3

commit v3 on v2

--- a/solution.py
+++ b/solution.py
@@ -421,7 +421,15 @@
         cluster_rescale_coefs[None, :],
         blender_result_matrix,
     )
-    mixed_a = lax.psum_scatter(partial_a, "tp", scatter_dimension=0, tiled=True)
+    tp_count = lax.axis_size("tp")
+    terms = lax.all_to_all(
+        partial_a.reshape(tp_count, tok_rows // tp_count, width_a),
+        "tp",
+        split_axis=0,
+        concat_axis=0,
+        tiled=True,
+    )
+    mixed_a = jnp.sum(terms.astype(jnp.float32), axis=0).astype(jnp.bfloat16)
     returned = returned.reshape(slot_total, -1)
     token_slots = slot_of.reshape(token_count, TOPK)
     combined = jnp.zeros((token_count, returned.shape[1]), jnp.float32)

time: 169 us -> 185 us (1.095)
  blocking collectives: 34.5 us -> 58.2 us
  waiting for transfers between devices: 50 us -> 40.4 us
    all_to_all x0 -> x1, blocking collectives: none -> 23.8 us  [local(): lax.all_to_all(partial_a.reshape(tp_count, tok_rows // tp_count, width_a)...]
    reduce_scatter x2, waiting for transfers between devices: 10.3 us -> 0.01 us  [local(): lax.psum_scatter(partials[k], 'tp', scatter_dimension=0, tiled=False)]
    all_to_all x2, waiting for transfers between devices: 12.7 us -> 22.4 us  [local(): lax.all_to_all(summed, 'ep', split_axis=0, concat_axis=0, tiled=True)]
    reduce_scatter x1 -> x0, waiting for transfers between devices: 9.06 us -> none  [local(): mixed_a = lax.psum_scatter(partial_a, 'tp', scatter_dimension=0, tiled=True)]
  transfers between devices with their start and end apart: 10 -> 9, of which waited for: 7 -> 5; matrix products, arithmetic and copies ran while one was open for 2% -> 2% of each run, Pallas kernels for 21% -> 19%
where the time goes in v3:
time: 185 us; the launch traced here: 184 us
  blocking collectives  58.2 us (31%)
  waiting for transfers between devices  40.4 us (22%)
  Pallas kernels  35.7 us (19%)
  starting transfers between devices  20.8 us (11%)
  between operations  14 us (8%)
  local copies, waits for them, and re-layouts  7.76 us (4%)
  other arithmetic  4.54 us (2%)
  matrix products  2.95 us (2%)
    all_to_all x2, blocking collectives, local(): lax.all_to_all(outgoing[:, :, k * size:(k + 1) * size], 'ep', split_axis=...  34.5 us
    all_to_all x1, blocking collectives, local(): lax.all_to_all(partial_a.reshape(tp_count, tok_rows // tp_count, width_a)...  23.8 us
    all_to_all x2, waiting for transfers between devices, local(): lax.all_to_all(summed, 'ep', split_axis=0, concat_axis=0, tiled=True)  22.4 us
    pallas_call x2, Pallas kernels, run_experts(): pl.pallas_call(experts_kernel, grid=(experts, units // tile), in_specs=[p...  20.7 us
    all_to_all x1, waiting for transfers between devices, local(): lax.all_to_all(pieces, 'ep', split_axis=0, concat_axis=0, tiled=True)  9.97 us
    all_to_all x2, starting transfers between devices, local(): lax.all_to_all(summed, 'ep', split_axis=0, concat_axis=0, tiled=True)  9.15 us
    all_to_all x1, waiting for transfers between devices, local(): lax.all_to_all(entering, 'ep', split_axis=0, concat_axis=0, tiled=True)  7.9 us
    unnamed x21, local copies, waits for them, and re-layouts  6.71 us
  transfers between devices with their start and end apart: 9, of which 5 were waited for; matrix products, arithmetic and copies ran while one was open for 2% of the time, Pallas kernels for 19%

profile of v3, /device:TPU:0, one launch (start us, length us, event | category | flops | bytes accessed | tf_op | source)
XLA Modules:
  0.0 184.4 jit_solution(768049442058446512)
XLA Ops:
  7.2 0.0 all-gather.5.cloned.1.call-start
  7.2 0.8 copy.57
  8.0 0.1 eq.60
  8.2 0.3 convert_reduce_fusion
  8.4 0.1 reduce_sum.45
  8.6 0.1 copy.58
  8.7 0.7 multiply_add_fusion
  9.4 0.3 fusion.4
  9.7 1.5 multiply_reduce_fusion
  11.2 0.8 dynamic-slice_convert_fusion
  12.0 1.4 convolution_convert_fusion
  13.4 0.1 fusion.11
  13.5 19.4 %all_to_all.35 = bf16[8,1,48,512]{3,2,1,0:T(8,128)(2,1)} all-to-all(bf16[8,1,48,512]{3,2,1,0:T(8,128)(2,1)S(1)} %get-tuple-element.26), channel_id=1, replica_groups=mesh['ep'=8,'tp'=4] {'ep'}, dimensions={0} | all-to-all | bytes 786432 | tf_op jit(solution)/shard_map/all_to_all | solution.py:346
  32.9 0.0 all-gather.5.cloned.1.call-update
  32.9 0.0 all-gather.3.cloned.1.call-start
  33.0 15.1 %all_to_all.36 = bf16[8,1,48,512]{3,2,1,0:T(8,128)(2,1)} all-to-all(bf16[8,1,48,512]{3,2,1,0:T(8,128)(2,1)S(1)} %get-tuple-element.27), channel_id=1, replica_groups=mesh['ep'=8,'tp'=4] {'ep'}, dimensions={0} | all-to-all | bytes 786432 | tf_op jit(solution)/shard_map/all_to_all | solution.py:346
  48.1 0.0 all-gather.3.cloned.1.call-update
  48.1 0.0 reduce-scatter.3.cloned.1.call-start
  48.2 3.0 %collective-permute-start = (bf16[8,2048]{1,0:T(8,128)(2,1)S(1)}, bf16[8,2048]{1,0:T(8,128)(2,1)S(1)}, u32[]{:S(2)}, u32[]{:S(2)}) collective-permute-start(bf16[8,2048]{1,0:T(8,128)(2,1)S(1)} %pad_maximum_fusion.1), channel_id=1, source_target_pairs={{0,4},{4,8},{8,12},{12,16},{16,20},{20,24},{24,28},{1,5},{5,9},{9,... | collective-permute-start | bytes 98312 | tf_op jit(solution)/shard_map/ppermute | solution.py:25
  51.2 0.8 copy.55.pre_ref
  51.9 0.8 copy.56.extra_ref
  52.7 0.1 collective-permute-done.rim_ref
  52.8 0.6 copy-done.8
  53.4 6.5 %ssd_local.1 = (f32[256,1024]{1,0:T(8,128)}, bf16[256,512]{1,0:T(8,128)(2,1)}, f32[256,16]{1,0:T(8,128)}, bf16[8,18,1024]{2,1,0:T(8,128)(2,1)}) custom-call(bf16[256,1024]{1,0:T(8,128)(2,1)} %x_ref.1, bf16[256,512]{1,0:T(8,128)(2,1)} %b_ref.1, bf16[256,512]{1,0:T(8,128)(2,1)} %c_ref.1, bf16[8,2048]{1,0:T(8,128)(2,1)} %copy-done.8, f32[256,16]{1,0:T(8,128)} %copy.55.pre_ref, ...), custom_call_target="tpu_custom_call" | custom-call | flops 8589934592 | bytes 3145728 | tf_op jit(solution)/shard_map/ssd_local/pallas_call | solution.py:281
  59.8 1.6 copy-done.1
  61.5 10.3 %experts.2 = bf16[4,1,384,512]{3,2,1,0:T(8,128)(2,1)} custom-call(bf16[4,1,384,512]{3,2,1,0:T(8,128)(2,1)S(1)} %copy-done.1, bf16[1,2048,1024]{2,1,0:T(8,128)(2,1)} %gate_ref.3, bf16[1,2048,1024]{2,1,0:T(8,128)(2,1)} %up_ref.3, bf16[1,1024,2048]{2,1,0:T(8,128)(2,1)} %down_ref.3), custom_call_target="tpu_custom_call" | custom-call | flops 4831838208 | bytes 15728640 | tf_op jit(solution)/shard_map/experts/pallas_call | solution.py:213
  71.8 4.7 %all-to-all-start.2 = ((bf16[8,18,1024]{2,1,0:T(8,128)(2,1)}), bf16[8,18,1024]{2,1,0:T(8,128)(2,1)S(1)}, u32[]{:S(2)}, u32[]{:S(2)}) async-start(bf16[8,18,1024]{2,1,0:T(8,128)(2,1)} %get-tuple-element.20), calls=%async_computation.2 | async-start | bytes 786432 | tf_op jit(solution)/shard_map/all_to_all | solution.py:370
  76.6 0.0 reduce-scatter.5.cloned.1.call-start
  76.6 0.0 all-gather.3.cloned.1.call-done.x_ref
  76.6 10.0 %all-to-all-done.2.in_ref = bf16[8,18,1024]{2,1,0:T(8,128)(2,1)S(1)} async-done(((bf16[8,18,1024]{2,1,0:T(8,128)(2,1)}), bf16[8,18,1024]{2,1,0:T(8,128)(2,1)S(1)}, u32[]{:S(2)}, u32[]{:S(2)}) %all-to-all-start.2) | async-done | bytes 294944 | tf_op jit(solution)/shard_map/all_to_all | solution.py:370
  86.6 1.4 copy-done
  88.0 10.4 %experts.3 = bf16[4,1,384,512]{3,2,1,0:T(8,128)(2,1)} custom-call(bf16[4,1,384,512]{3,2,1,0:T(8,128)(2,1)S(1)} %copy-done, bf16[1,2048,1024]{2,1,0:T(8,128)(2,1)} %gate_ref.3, bf16[1,2048,1024]{2,1,0:T(8,128)(2,1)} %up_ref.3, bf16[1,1024,2048]{2,1,0:T(8,128)(2,1)} %down_ref.3), custom_call_target="tpu_custom_call" | custom-call | flops 4831838208 | bytes 15728640 | tf_op jit(solution)/shard_map/experts/pallas_call | solution.py:213
  98.4 0.0 reduce-scatter.5.cloned.1.call-update
  98.5 1.8 state_prefix.1
  100.3 3.7 %all-to-all-start.3 = ((bf16[8,16,1024]{2,1,0:T(8,128)(2,1)}), bf16[8,16,1024]{2,1,0:T(8,128)(2,1)S(1)}, u32[]{:S(2)}, u32[]{:S(2)}) async-start(bf16[8,16,1024]{2,1,0:T(8,128)(2,1)} %state_prefix.1), calls=%async_computation.3 | async-start | bytes 524288 | tf_op jit(solution)/shard_map/all_to_all | solution.py:387
  104.0 0.6 broadcast_in_dim.11.gain_ref
  104.6 7.9 %all-to-all-done.3 = bf16[8,16,1024]{2,1,0:T(8,128)(2,1)S(1)} async-done(((bf16[8,16,1024]{2,1,0:T(8,128)(2,1)}), bf16[8,16,1024]{2,1,0:T(8,128)(2,1)S(1)}, u32[]{:S(2)}, u32[]{:S(2)}) %all-to-all-start.3) | async-done | bytes 262176 | tf_op jit(solution)/shard_map/all_to_all | solution.py:387
  112.5 0.7 copy-done.3
  113.2 6.7 %finish_mixer.1 = bf16[256,2048]{1,0:T(8,128)(2,1)} custom-call(f32[256,1024]{1,0:T(8,128)} %get-tuple-element.14.y_ref, bf16[256,512]{1,0:T(8,128)(2,1)} %get-tuple-element.15.cc_ref, f32[256,16]{1,0:T(8,128)} %get-tuple-element.16.run_ref, bf16[128,1024]{1,0:T(8,128)(2,1)} %bitcast.33, bf16[256,1024]{1,0:T(8,128)(2,1)} %valve_ref.1, ...), custom_call_target="tpu_custom_call" | custom-call | flops 5368709120 | bytes 7340032 | tf_op jit(solution)/shard_map/finish_mixer/pallas_call | solution.py:393
  119.9 23.8 %all_to_all.37 = bf16[4,64,2048]{2,1,0:T(8,128)(2,1)S(1)} all-to-all(bf16[4,64,2048]{2,1,0:T(8,128)(2,1)} %bitcast.30), channel_id=1, replica_groups=mesh['ep'=8,'tp'=4] {'tp'}, dimensions={0} | all-to-all | bytes 2097152 | tf_op jit(solution)/shard_map/all_to_all | solution.py:425
  143.7 5.5 %all-to-all-start.5 = ((bf16[8,1,48,512]{3,2,1,0:T(8,128)(2,1)}), bf16[8,1,48,512]{3,2,1,0:T(8,128)(2,1)S(1)}, u32[]{:S(2)}, u32[]{:S(2)}) async-start(bf16[8,1,48,512]{3,2,1,0:T(8,128)(2,1)} %bitcast.31), calls=%async_computation.6 | async-start | bytes 786432 | tf_op jit(solution)/shard_map/all_to_all | solution.py:378
  149.2 11.7 %all-to-all-done.5 = bf16[8,1,48,512]{3,2,1,0:T(8,128)(2,1)S(1)} async-done(((bf16[8,1,48,512]{3,2,1,0:T(8,128)(2,1)}), bf16[8,1,48,512]{3,2,1,0:T(8,128)(2,1)S(1)}, u32[]{:S(2)}, u32[]{:S(2)}) %all-to-all-start.5) | async-done | bytes 393248 | tf_op jit(solution)/shard_map/all_to_all | solution.py:378
  160.9 3.6 %all-to-all-start.6 = ((bf16[8,1,48,512]{3,2,1,0:T(8,128)(2,1)}), bf16[8,1,48,512]{3,2,1,0:T(8,128)(2,1)S(1)}, u32[]{:S(2)}, u32[]{:S(2)}) async-start(bf16[8,1,48,512]{3,2,1,0:T(8,128)(2,1)} %bitcast.32), calls=%async_computation.8 | async-start | bytes 786432 | tf_op jit(solution)/shard_map/all_to_all | solution.py:378
  164.6 0.9 reduce_sum.48
  165.5 10.7 %all-to-all-done.6 = bf16[8,1,48,512]{3,2,1,0:T(8,128)(2,1)S(1)} async-done(((bf16[8,1,48,512]{3,2,1,0:T(8,128)(2,1)}), bf16[8,1,48,512]{3,2,1,0:T(8,128)(2,1)S(1)}, u32[]{:S(2)}, u32[]{:S(2)}) %all-to-all-start.6) | async-done | bytes 393248 | tf_op jit(solution)/shard_map/all_to_all | solution.py:378
  176.2 0.1 pad_maximum_fusion
  176.3 0.4 convolution_multiply_fusion.1
  176.7 1.1 fusion.2
  (28 shorter events, 0.1 us)
Async XLA Ops:
  7.2 52.7 %all-gather.5.cloned.1.call-start = ((), (), s32[]{:S(2)}) async-start(), calls=%async_computation.10 | async-start | bytes 1966080 | tf_op jit(solution)/shard_map/all_gather | solution.py:354
  13.5 34.7 %slice-start = ((bf16[256,1024]{1,0:T(8,128)(2,1)}), bf16[8,1024]{1,0:T(8,128)(2,1)S(1)}, s32[]{:S(2)}) async-start(bf16[256,1024]{1,0:T(8,128)(2,1)} %x_ref.1), calls=%async_computation.13 | async-start | bytes 32768 | tf_op jit(solution)/shard_map/slice | solution.py:272
  13.5 34.7 %slice-start.1 = ((bf16[256,512]{1,0:T(8,128)(2,1)}), bf16[8,512]{1,0:T(8,128)(2,1)S(1)}, s32[]{:S(2)}) async-start(bf16[256,512]{1,0:T(8,128)(2,1)} %c_ref.1), calls=%async_computation.14 | async-start | bytes 16384 | tf_op jit(solution)/shard_map/slice | solution.py:274
  13.5 34.7 %slice-start.2 = ((bf16[256,512]{1,0:T(8,128)(2,1)}), bf16[8,512]{1,0:T(8,128)(2,1)S(1)}, s32[]{:S(2)}) async-start(bf16[256,512]{1,0:T(8,128)(2,1)} %b_ref.1), calls=%async_computation.15 | async-start | bytes 16384 | tf_op jit(solution)/shard_map/slice | solution.py:273
  13.5 37.7 %copy-start.4 = (f32[256,16]{0,1:T(8,128)S(1)}, f32[256,16]{0,1:T(8,128)}, u32[]{:S(2)}) copy-start(f32[256,16]{0,1:T(8,128)} %param.25) | copy-start | bytes 49156
  13.5 38.4 %copy-start.5 = (f32[256,16]{0,1:T(8,128)S(1)}, f32[256,16]{0,1:T(8,128)}, u32[]{:S(2)}) copy-start(f32[256,16]{0,1:T(8,128)} %param.26) | copy-start | bytes 49156
  32.9 43.7 %all-gather.3.cloned.1.call-start = ((), (), s32[]{:S(2)}) async-start(), calls=%async_computation.9 | async-start | bytes 1966080 | tf_op jit(solution)/shard_map/all_gather | solution.py:354
  48.1 95.6 %reduce-scatter.3.cloned.1.call-start = ((), (), s32[]{:S(2)}) async-start(), calls=%async_computation.11 | async-start | bytes 1966080 | tf_op jit(solution)/shard_map/reduce_scatter | solution.py:376
  48.2 4.6 %collective-permute-start = (bf16[8,2048]{1,0:T(8,128)(2,1)S(1)}, bf16[8,2048]{1,0:T(8,128)(2,1)S(1)}, u32[]{:S(2)}, u32[]{:S(2)}) collective-permute-start(bf16[8,2048]{1,0:T(8,128)(2,1)S(1)} %pad_maximum_fusion.1), channel_id=1, source_target_pairs={{0,4},{4,8},{8,12},{12,16},{16,20},{20,24},{24,28},{1,5},{5,9},{9,... | collective-permute-start | bytes 98312 | tf_op jit(solution)/shard_map/ppermute | solution.py:25
  52.8 0.6 copy-start.8
  59.8 1.6 copy-start.1
  71.8 14.8 %all-to-all-start.2 = ((bf16[8,18,1024]{2,1,0:T(8,128)(2,1)}), bf16[8,18,1024]{2,1,0:T(8,128)(2,1)S(1)}, u32[]{:S(2)}, u32[]{:S(2)}) async-start(bf16[8,18,1024]{2,1,0:T(8,128)(2,1)} %get-tuple-element.20), calls=%async_computation.2 | async-start | bytes 786432 | tf_op jit(solution)/shard_map/all_to_all | solution.py:370
  76.6 72.7 %reduce-scatter.5.cloned.1.call-start = ((), (), s32[]{:S(2)}) async-start(), calls=%async_computation.12 | async-start | bytes 1966080 | tf_op jit(solution)/shard_map/reduce_scatter | solution.py:376
  86.6 1.4 copy-start
  88.0 10.4 %copy-start.2 = (bf16[8,18,1024]{2,1,0:T(8,128)(2,1)}, bf16[8,18,1024]{2,1,0:T(8,128)(2,1)S(1)}, u32[]{:S(2)}) copy-start(bf16[8,18,1024]{2,1,0:T(8,128)(2,1)S(1)} %all-to-all-done.2.in_ref) | copy-start | bytes 884740
  98.4 5.6 %copy-start.6 = (bf16[1024]{0:T(1024)(128)(2,1)S(1)}, bf16[1024]{0:T(1024)(128)(2,1)}, u32[]{:S(2)}) copy-start(bf16[1024]{0:T(1024)(128)(2,1)} %param.33) | copy-start | bytes 6148
  100.3 12.2 %all-to-all-start.3 = ((bf16[8,16,1024]{2,1,0:T(8,128)(2,1)}), bf16[8,16,1024]{2,1,0:T(8,128)(2,1)S(1)}, u32[]{:S(2)}, u32[]{:S(2)}) async-start(bf16[8,16,1024]{2,1,0:T(8,128)(2,1)} %state_prefix.1), calls=%async_computation.3 | async-start | bytes 524288 | tf_op jit(solution)/shard_map/all_to_all | solution.py:387
  112.5 0.7 copy-start.3
  119.9 44.7 %copy-start.7 = (f32[256,2]{0,1:T(2,128)S(1)}, f32[256,2]{0,1:T(2,128)}, u32[]{:S(2)}) copy-start(f32[256,2]{0,1:T(2,128)} %param.41) | copy-start | bytes 6148
  143.7 17.2 %all-to-all-start.5 = ((bf16[8,1,48,512]{3,2,1,0:T(8,128)(2,1)}), bf16[8,1,48,512]{3,2,1,0:T(8,128)(2,1)S(1)}, u32[]{:S(2)}, u32[]{:S(2)}) async-start(bf16[8,1,48,512]{3,2,1,0:T(8,128)(2,1)} %bitcast.31), calls=%async_computation.6 | async-start | bytes 786432 | tf_op jit(solution)/shard_map/all_to_all | solution.py:378
  160.9 15.3 %all-to-all-start.6 = ((bf16[8,1,48,512]{3,2,1,0:T(8,128)(2,1)}), bf16[8,1,48,512]{3,2,1,0:T(8,128)(2,1)S(1)}, u32[]{:S(2)}, u32[]{:S(2)}) async-start(bf16[8,1,48,512]{3,2,1,0:T(8,128)(2,1)} %bitcast.32), calls=%async_computation.8 | async-start | bytes 786432 | tf_op jit(solution)/shard_map/all_to_all | solution.py:378
Sparse Core Ops, SparseCore 0:
  33.0 18.3 all-gather.4
  53.0 19.6 all-gather.2
  75.2 27.9 reduce-scatter.2
  105.6 33.7 reduce-scatter.4
